TPU v7x, 32 devices: a whole 2x2x4 slice. The times are simulated.
32 devices in a mesh: grp: 2 (over y), sp: 4 (over z), tp: 4 (over x, core).
Axes of the slice: x: 2, y: 2, z: 4, core: 2. Of those that a mesh axis runs over, the one named last changes fastest.
Arguments:
- latent: bfloat16 [12288, 2048], P(('grp', 'sp')), parts along dimension 0, may hold values from -6 to 6
- condition: bfloat16 [4096], P('grp'), parts along dimension 0, may hold values from -6 to 6
- context_tokens: bfloat16 [512, 2048], P(('grp', 'sp')), parts along dimension 0, may hold values from -6 to 6
- context_condition: bfloat16 [2048], replicated, may hold values from -6 to 6
- shift_weight: bfloat16 [2048, 2048], P('sp', 'tp'), may hold values from -0.25 to 0.25
- scale_weight: bfloat16 [2048, 2048], P('sp', 'tp'), may hold values from -0.25 to 0.25
- gate_weight: bfloat16 [2048, 2048], P('sp', 'tp'), may hold values from -0.25 to 0.25
- norm_gain: bfloat16 [2048], replicated, may hold values from 0.099609375 to 1.8984375
- query_weight: bfloat16 [2048, 1024], P(None, 'tp'), may hold values from -0.125 to 0.125
- key_weight: bfloat16 [2048, 1024], P(None, 'tp'), may hold values from -0.125 to 0.125
- value_weight: bfloat16 [2048, 1024], P(None, 'tp'), may hold values from -0.125 to 0.125
- out_weight: bfloat16 [1024, 2048], replicated, may hold values from -0.1875 to 0.1875
- offset_bias: float32 [16, 15, 31], P('tp'), may hold values from 0.5 to 260
Outputs:
- mixed_latent: bfloat16 [12288, 2048], P(('grp', 'sp', 'tp')), parts along dimension 0
There are 2 independent parts, one for each index of `grp`. A program takes and returns all parts, laid end to end along the dimension named above; an argument that names none is the same for every part. Nothing has to cross between parts.
All inputs are finite; a program needn't handle non-finite values.
Results may differ from a plain program's by a relative error of at most 0.011.
Values may be sent and summed in bfloat16 or wider, within the bound.
A program may use at most 192 MiB of HBM per device.

v0:
```python
import functools

import jax
import jax.numpy as jnp
from jax import lax
from jax.experimental import pallas as pl
from jax.experimental.pallas import tpu as pltpu
from jax.sharding import PartitionSpec as P

HEAD_DIM = 64
GRID_W = 64
WIN_ROWS = 8
WIN_COLS = 16
HALO = WIN_ROWS // 2
epsilon = 1e-06
masked_score = -1e30
F32 = jnp.float32
BF16 = jnp.bfloat16
MESH = pl.DeviceIdType.MESH


def whole_spec(shape):
    return pl.BlockSpec(shape, lambda *_: (0,) * len(shape))


def to_peer(src, dst, send, recv, **place):
    return pltpu.make_async_remote_copy(
        src_ref=src, dst_ref=dst, send_sem=send, recv_sem=recv,
        device_id=place, device_id_type=MESH,
    )


def front_kernel(
    small_ref, shift_w, scale_w, gate_w,
    ctx_hbm, lat_hbm, wq_hbm, wk_hbm, wv_hbm,
    q_ref, kv_ref, ctx_out, gate_ref,
    terms, arrived, vectors, lat, ctx, wq, wk, wv,
    load_sem, term_send, term_recv, halo_send, halo_recv, ctx_send, ctx_recv,
):
    sp, tp = lax.axis_index("sp"), lax.axis_index("tp")
    sp_size, tp_size = lax.axis_size("sp"), lax.axis_size("tp")
    group = sp_size * tp_size
    me = sp * tp_size + tp
    input_rows, piece = shift_w.shape
    tokens, width = q_ref.shape
    context_rows = ctx.shape[0]
    halo = HALO * GRID_W
    tiles = tokens // halo

    def peer(d):
        other = (me + d) % group
        return dict(sp=other // tp_size, tp=other % tp_size)

    barrier = pltpu.get_barrier_semaphore()

    @pl.loop(1, group)
    def _(d):
        pl.semaphore_signal(barrier, inc=1, device_id=peer(d), device_id_type=MESH)

    loads = [
        pltpu.make_async_copy(ctx_hbm, ctx, load_sem.at[0]),
        pltpu.make_async_copy(wk_hbm, wk, load_sem.at[1]),
        pltpu.make_async_copy(wv_hbm, wv, load_sem.at[2]),
        pltpu.make_async_copy(wq_hbm, wq, load_sem.at[3]),
        pltpu.make_async_copy(lat_hbm, lat, load_sem.at[4]),
    ]
    for load in loads:
        load.start()

    depth = sp_size * input_rows

    def own(i):
        start = pl.multiple_of(i * depth + sp * input_rows, input_rows)
        return small_ref[:, pl.ds(start, input_rows)]

    row = lax.broadcasted_iota(jnp.int32, (8, input_rows), 0)
    value = jnp.where(row == 0, own(0), own(1))
    act = (value / (1.0 + jnp.exp(-value))).astype(BF16)
    terms[...] = jnp.zeros_like(terms)
    for i, w in enumerate((shift_w, scale_w, gate_w)):
        terms[2 * i : 2 * i + 2, :] = jnp.dot(act, w[...], preferred_element_type=F32)[:2]
    arrived[me] = terms[...]
    pl.semaphore_wait(barrier, group - 1)

    def term_copy(d):
        return to_peer(terms, arrived.at[me], term_send.at[d], term_recv.at[d], **peer(d))

    @pl.loop(1, group)
    def _(d):
        term_copy(d).start()

    for load in loads:
        load.wait()

    @pl.loop(1, group)
    def _(d):
        term_copy(d).wait()

    for t in range(tp_size):
        total = arrived[t]
        for s in range(1, sp_size):
            total = total + arrived[s * tp_size + t]
        vectors[:, t * piece : (t + 1) * piece] = total
    gate_ref[...] = vectors[4:5, :]

    def hidden_of(x, which):
        x = x.astype(F32)
        inverse = lax.rsqrt(jnp.mean(x * x, axis=-1, keepdims=True) + epsilon)
        factor = small_ref[:, 2 * depth :] * (1.0 + vectors[2 + which : 3 + which, :])
        return (x * inverse * factor + vectors[which : which + 1, :]).astype(BF16)

    def pairs_of(hidden, out, rows):
        out[rows, :width] = jnp.dot(hidden, wk[...], preferred_element_type=F32).astype(BF16)
        out[rows, width:] = jnp.dot(hidden, wv[...], preferred_element_type=F32).astype(BF16)

    def tile(i):
        start = pl.multiple_of(i * halo, halo)
        hidden = hidden_of(lat[pl.ds(start, halo), :], 0)
        pairs_of(hidden, kv_ref, pl.ds(pl.multiple_of(start + halo, halo), halo))
        q = jnp.dot(hidden, wq[...], preferred_element_type=F32)
        q_ref[pl.ds(start, halo), :] = (q * HEAD_DIM**-0.5).astype(BF16)

    ctx_rows = pl.ds(pl.multiple_of(sp * context_rows, context_rows), context_rows)
    pairs_of(hidden_of(ctx[...], 1), ctx_out, ctx_rows)

    def ctx_copy(d):
        return to_peer(
            ctx_out.at[ctx_rows], ctx_out.at[ctx_rows], ctx_send.at[d], ctx_recv.at[d],
            sp=(sp + d) % sp_size, tp=tp,
        )

    down = to_peer(
        kv_ref.at[pl.ds(halo, halo)], kv_ref.at[pl.ds(halo + tokens, halo)],
        halo_send.at[0], halo_recv.at[0], sp=jnp.maximum(sp - 1, 0), tp=tp,
    )
    up = to_peer(
        kv_ref.at[pl.ds(tokens, halo)], kv_ref.at[pl.ds(0, halo)],
        halo_send.at[1], halo_recv.at[1], sp=jnp.minimum(sp + 1, sp_size - 1), tp=tp,
    )
    tile(0)

    @pl.when(sp > 0)
    def _():
        down.start()

    tile(tiles - 1)

    @pl.when(sp < sp_size - 1)
    def _():
        up.start()

    @pl.loop(1, sp_size)
    def _(d):
        ctx_copy(d).start()

    @pl.loop(1, tiles - 1)
    def _(i):
        tile(i)

    @pl.when(sp > 0)
    def _():
        down.wait_send()
        up.wait_recv()

    @pl.when(sp < sp_size - 1)
    def _():
        up.wait_send()
        down.wait_recv()

    @pl.loop(1, sp_size)
    def _(d):
        ctx_copy(d).wait()


def front(
    small, shift_w, scale_w, gate_w, context_tokens, latent, wq, wk, wv
):
    sp_size, tp_size = lax.axis_size("sp"), lax.axis_size("tp")
    group = sp_size * tp_size
    piece = shift_w.shape[1]
    tokens, depth = latent.shape
    context_rows = context_tokens.shape[0]
    width = wq.shape[1]
    padded = tokens + 2 * HALO * GRID_W
    vmem = pl.BlockSpec(memory_space=pltpu.VMEM)
    hbm = pl.BlockSpec(memory_space=pl.ANY)
    dma = pltpu.SemaphoreType.DMA
    return pl.pallas_call(
        front_kernel,
        in_specs=[vmem] * 4 + [hbm] * 5,
        out_specs=[vmem] * 4,
        out_shape=[
            jax.ShapeDtypeStruct((tokens, width), BF16),
            jax.ShapeDtypeStruct((padded, 2 * width), BF16),
            jax.ShapeDtypeStruct((sp_size * context_rows, 2 * width), BF16),
            jax.ShapeDtypeStruct((1, depth), F32),
        ],
        scratch_shapes=[
            pltpu.VMEM((8, piece), F32),
            pltpu.VMEM((group, 8, piece), F32),
            pltpu.VMEM((8, depth), F32),
            pltpu.VMEM((tokens, depth), BF16),
            pltpu.VMEM((context_rows, depth), BF16),
            pltpu.VMEM((depth, width), BF16),
            pltpu.VMEM((depth, width), BF16),
            pltpu.VMEM((depth, width), BF16),
            dma((5,)), dma((group,)), dma((group,)), dma((2,)), dma((2,)),
            dma((sp_size,)), dma((sp_size,)),
        ],
        compiler_params=pltpu.CompilerParams(
            vmem_limit_bytes=58 * 2**20, collective_id=0, has_side_effects=True
        ),
        cost_estimate=pl.CostEstimate(
            flops=6 * tokens * depth * width,
            bytes_accessed=2 * (tokens * depth + 3 * depth * width + 3 * tokens * width),
            transcendentals=0,
        ),
    )(small, shift_w, scale_w, gate_w, context_tokens, latent, wq, wk, wv)


def build_bias(bias_ref, table, heads):
    lane = lax.broadcasted_iota(jnp.int32, (GRID_W, 2 * GRID_W), 1)
    query = lax.broadcasted_iota(jnp.int32, (GRID_W, 2 * GRID_W), 0)
    column = jnp.where(lane >= GRID_W, lane - GRID_W, lane)
    first = jnp.clip(query - WIN_COLS // 2, 0, GRID_W - WIN_COLS)
    inside = (column >= first) & (column < first + WIN_COLS)
    wide = 2 * GRID_W

    def one(row, base):
        spread = jnp.broadcast_to(row, (GRID_W, wide))
        return pltpu.roll(spread, (base - (WIN_COLS - 1)) % wide, 1, stride=1, stride_axis=0)

    for h in range(heads):
        low = one(bias_ref[h, 0:1, :], 0)
        for o in range(2 * WIN_ROWS - 2):
            row = bias_ref[h, o + 1 : o + 2, :]
            both = jnp.where(lane < GRID_W, low, one(row, GRID_W))
            table[o, h * GRID_W : (h + 1) * GRID_W, :] = jnp.where(inside, both, masked_score)
            low = one(row, 0)


def attend_kernel(
    heads, q_hbm, kv_hbm, ctx_hbm, bias_ref, out_ref,
    q_ref, kv, ctx_ref, stage, table, load_sem, send_sem, recv_sem,
):
    tokens, width = q_ref.shape
    grid_rows = tokens // GRID_W
    sp, tp = lax.axis_index("sp"), lax.axis_index("tp")
    tp_size = lax.axis_size("tp")
    total_rows = grid_rows * lax.axis_size("sp")
    share = tokens // tp_size
    share_rows = share // GRID_W

    barrier = pltpu.get_barrier_semaphore()

    @pl.loop(1, tp_size)
    def _(d):
        pl.semaphore_signal(
            barrier, inc=1, device_id=dict(tp=(tp + d) % tp_size), device_id_type=MESH
        )

    loads = [
        pltpu.make_async_copy(kv_hbm, kv, load_sem.at[0]),
        pltpu.make_async_copy(q_hbm, q_ref, load_sem.at[1]),
        pltpu.make_async_copy(ctx_hbm, ctx_ref, load_sem.at[2]),
    ]
    for load in loads:
        load.start()
    build_bias(bias_ref, table, heads)
    pl.semaphore_wait(barrier, tp_size - 1)
    for load in loads:
        load.wait()

    contract = (((1,), (1,)), ((), ()))
    head_of = lax.broadcasted_iota(jnp.int32, (GRID_W, width), 1) // HEAD_DIM

    def one_row(local_row):
        row = sp * grid_rows + local_row
        first = jnp.clip(row - HALO, 0, total_rows - WIN_ROWS)
        start = pl.multiple_of((first - sp * grid_rows + HALO) * GRID_W, GRID_W)
        offset = first - row + WIN_ROWS - 1
        place = pl.ds(pl.multiple_of(local_row * GRID_W, GRID_W), GRID_W)
        q = q_ref[place, :]
        stacked = jnp.concatenate(
            [jnp.where(head_of == h, q, jnp.zeros_like(q)) for h in range(heads)], axis=0
        )
        near = lax.dot_general(
            stacked, kv[pl.ds(start, WIN_ROWS * GRID_W), :width], contract,
            preferred_element_type=F32,
        )
        far = lax.dot_general(stacked, ctx_ref[:, :width], contract, preferred_element_type=F32)
        near = near + jnp.concatenate(
            [table[offset + 2 * w] for w in range(WIN_ROWS // 2)], axis=1
        )
        peak = jnp.maximum(
            jnp.max(near, axis=1, keepdims=True), jnp.max(far, axis=1, keepdims=True)
        )
        near = jnp.exp(near - peak)
        far = jnp.exp(far - peak)
        total = jnp.sum(near, axis=1, keepdims=True) + jnp.sum(far, axis=1, keepdims=True)
        mixed = jnp.dot(
            near.astype(BF16), kv[pl.ds(start, WIN_ROWS * GRID_W), width:],
            preferred_element_type=F32,
        ) + jnp.dot(far.astype(BF16), ctx_ref[:, width:], preferred_element_type=F32)
        mixed = mixed * (1.0 / total)
        merged = mixed[:GRID_W]
        for h in range(1, heads):
            merged = jnp.where(head_of == h, mixed[h * GRID_W : (h + 1) * GRID_W], merged)
        stage[place, :] = merged.astype(BF16)

    def rows_of(owner):
        return pl.ds(pl.multiple_of(owner * share, share), share)

    def chunk_copy(d):
        owner = (tp + d) % tp_size
        return to_peer(
            stage.at[rows_of(owner)], out_ref.at[tp], send_sem.at[d], recv_sem.at[d], tp=owner
        )

    def chunk(d):
        owner = (tp + d) % tp_size
        for i in range(share_rows):
            one_row(owner * share_rows + i)

    @pl.loop(1, tp_size)
    def _(d):
        chunk(d)
        chunk_copy(d).start()

    chunk(0)
    out_ref[tp] = stage[rows_of(tp), :]

    @pl.loop(1, tp_size)
    def _(d):
        chunk_copy(d).wait()


def attend(q, kv, ctx, bias):
    tokens, width = q.shape
    heads = bias.shape[0]
    tp_size = lax.axis_size("tp")
    vmem = pl.BlockSpec(memory_space=pltpu.VMEM)
    keys = WIN_ROWS * GRID_W + ctx.shape[0]
    return pl.pallas_call(
        functools.partial(attend_kernel, heads),
        in_specs=[pl.BlockSpec(memory_space=pl.ANY)] * 3 + [vmem],
        out_specs=vmem,
        out_shape=jax.ShapeDtypeStruct((tp_size, tokens // tp_size, width), BF16),
        scratch_shapes=[
            pltpu.VMEM(q.shape, BF16),
            pltpu.VMEM(kv.shape, BF16),
            pltpu.VMEM(ctx.shape, BF16),
            pltpu.VMEM((tokens, width), BF16),
            pltpu.VMEM((2 * WIN_ROWS - 2, heads * GRID_W, 2 * GRID_W), F32),
            pltpu.SemaphoreType.DMA((3,)),
            pltpu.SemaphoreType.DMA((tp_size,)),
            pltpu.SemaphoreType.DMA((tp_size,)),
        ],
        compiler_params=pltpu.CompilerParams(
            vmem_limit_bytes=58 * 2**20, collective_id=1, has_side_effects=True
        ),
        cost_estimate=pl.CostEstimate(
            flops=4 * tokens * heads * width * keys,
            bytes_accessed=12 * tokens * width,
            transcendentals=tokens * heads * keys,
        ),
    )(q, kv, ctx, bias)


def local(
    latent, condition, context_tokens, context_condition, shift_weight, scale_weight,
    gate_weight, norm_gain, query_weight, key_weight, value_weight, out_weight, offset_bias,
):
    tp_index = lax.axis_index("tp")
    tp_size = lax.axis_size("tp")
    queries, pairs, context_all, gate = front(
        jnp.concatenate([condition, context_condition, norm_gain]).astype(F32)[None, :], shift_weight, scale_weight, gate_weight,
        context_tokens, latent, query_weight, key_weight, value_weight,
    )
    bias = jnp.pad(
        offset_bias,
        ((0, 0), (0, 1), (0, 2 * GRID_W - offset_bias.shape[2])),
    )
    exchanged = attend(queries, pairs, context_all, bias)
    share, width = exchanged.shape[1:]
    branch = jnp.einsum(
        "tnd,tde->ne",
        exchanged,
        out_weight.reshape(tp_size, width, out_weight.shape[1]),
        preferred_element_type=F32,
    )
    own_latent = lax.dynamic_slice_in_dim(latent, tp_index * share, share, 0)
    return (own_latent.astype(F32) + gate * branch).astype(BF16)


def solution(mesh):
    placed = (
        P(("grp", "sp"), None),
        P("grp"),
        P(("grp", "sp"), None),
        P(),
        P("sp", "tp"),
        P("sp", "tp"),
        P("sp", "tp"),
        P(),
        P(None, "tp"),
        P(None, "tp"),
        P(None, "tp"),
        P(),
        P("tp", None, None),
    )
    return jax.shard_map(
        local, mesh=mesh, in_specs=placed, out_specs=P(("grp", "sp", "tp"), None), check_vma=False
    )
```

profile of v0, /device:TPU:25, one launch (start us, length us, event | category | flops | bytes accessed | tf_op | source)
XLA Modules:
  0.0 55.1 jit_solution(14088001106907460749)
XLA Ops:
  0.0 0.7 %concatenate.16 = bf16[1,2048]{1,0:T(2,128)(2,1)S(1)} reshape(bf16[2048]{0:T(1024)(128)(2,1)} %param.14) | data formatting | bytes 8192 | tf_op jit(solution)/shard_map/concatenate | solution.py:377
  0.7 0.7 %concatenate.17 = bf16[1,2048]{1,0:T(2,128)(2,1)S(1)} reshape(bf16[2048]{0:T(1024)(128)(2,1)} %param.16) | data formatting | bytes 8192 | tf_op jit(solution)/shard_map/concatenate | solution.py:377
  1.4 0.7 %concatenate.18 = bf16[1,2048]{1,0:T(2,128)(2,1)S(1)} reshape(bf16[2048]{0:T(1024)(128)(2,1)} %param.20) | data formatting | bytes 8192 | tf_op jit(solution)/shard_map/concatenate | solution.py:377
  2.1 0.6 %maximum_convert_fusion.small_ref = f32[1,6144]{1,0:T(1,128)} fusion(bf16[1,2048]{1,0:T(2,128)(2,1)S(1)} %concatenate.18, bf16[1,2048]{1,0:T(2,128)(2,1)S(1)} %concatenate.17, bf16[1,2048]{1,0:T(2,128)(2,1)S(1)} %concatenate.16), kind=kLoop, calls=%fused_computation.3 | loop fusion | flops 36864 | bytes 36864 | tf_op jit(solution)/shard_map/convert_element_type | solution.py:377
  2.7 0.0 copy-start
  2.7 28.8 %shard_map.127 = (bf16[1536,256]{1,0:T(8,128)(2,1)}, bf16[2048,512]{1,0:T(8,128)(2,1)}, bf16[256,512]{1,0:T(8,128)(2,1)}, f32[1,2048]{1,0:T(1,128)}) custom-call(f32[1,6144]{1,0:T(1,128)} %maximum_convert_fusion.small_ref, bf16[512,512]{1,0:T(8,128)(2,1)} %shift_w.1, bf16[512,512]{1,0:T(8,128)(2,1)} %scale_w.1, bf16[512,512]{1,0:T(8,128)(2,1)} %gate_w.1, ...), custom_call_target="tpu_custom_call" | custom-call | flops 4831838208 | bytes 11796480 | tf_op jit(solution)/shard_map/pallas_call | solution.py:188
  31.5 0.0 copy-done
  31.5 0.6 %pad.4.bias_ref = f32[4,16,128]{2,1,0:T(8,128)} pad(f32[4,15,31]{2,1,0:T(8,128)S(1)} %copy.14, f32[]{:T(128)} %constant.11.clone.1), padding=0_0x0_1x0_97 | pad | bytes 40212 | tf_op jit(solution)/shard_map/jit(_pad)/pad | solution.py:380
  32.1 0.0 copy-start.1
  32.1 17.1 %shard_map.128 = bf16[4,384,256]{2,1,0:T(8,128)(2,1)} custom-call(bf16[1536,256]{1,0:T(8,128)(2,1)} %get-tuple-element.10.q_hbm, bf16[2048,512]{1,0:T(8,128)(2,1)} %get-tuple-element.11.kv_hbm, bf16[256,512]{1,0:T(8,128)(2,1)} %get-tuple-element.12.ctx_hbm, f32[4,16,128]{2,1,0:T(8,128)} %pad.4.bias_ref), custom_call_target="tpu_custom_call" | custom-call | flops 4831838208 | bytes 4718592 | tf_op jit(solution)/shard_map/pallas_call | solution.py:344
  49.2 0.0 copy-done.1
  49.2 5.9 %fusion.1 = bf16[384,2048]{1,0:T(8,128)(2,1)} fusion(bf16[4,384,256]{2,1,0:T(8,128)(2,1)} %shard_map.128, bf16[4,256,2048]{2,1,0:T(8,128)(2,1)} %bitcast.10, f32[2048]{0:T(1024)S(1)} %bitcast.11, bf16[1536,2048]{1,0:T(8,128)(2,1)} %lat_hbm.1, s32[]{:T(128)S(6)} %select_n.3), kind=kOutput, calls=%fused_computation.2 | convolution fusion | flops 1613758464 | bytes 8134660 | tf_op jit(solution)/shard_map/tnd,tde->ne/dot_general | solution.py:386
  (1 shorter events, 0.0 us)
Async XLA Ops:
  2.7 28.8 %copy-start = (f32[4,15,31]{2,0,1:T(4,128)S(1)}, f32[4,15,31]{2,0,1:T(4,128)}, u32[]{:S(2)}) copy-start(f32[4,15,31]{2,0,1:T(4,128)} %param.25) | copy-start | bytes 22324
  32.1 17.1 %copy-start.1 = (f32[1,2048]{1,0:T(1,128)S(1)}, f32[1,2048]{1,0:T(1,128)}, u32[]{:S(2)}) copy-start(f32[1,2048]{1,0:T(1,128)} %get-tuple-element.9) | copy-start | bytes 24580
where the time goes:
time: 55.4 us; the launch traced here: 55.1 us
  Pallas kernels  45.8 us (83%)
  matrix products  5.86 us (11%)
  local copies, waits for them, and re-layouts  2.71 us (5%)
  other arithmetic  0.63 us (1%)
    pallas_call x1, Pallas kernels, front(): pl.pallas_call(front_kernel, in_specs=[vmem] * 4 + [hbm] * 5, out_specs=[...  28.8 us
    pallas_call x1, Pallas kernels, attend(): pl.pallas_call(functools.partial(attend_kernel, heads), in_specs=[pl.Bloc...  17.1 us
    dot_general x1, matrix products, local(): jnp.einsum('tnd,tde->ne', exchanged, out_weight.reshape(tp_size, width, o...  5.86 us
    concatenate x3, local copies, waits for them, and re-layouts, local(): jnp.concatenate([condition, context_condition, norm_gain]).astype(F32)  2.08 us

commit v1 on v0

v1 whole, which is shorter than its diff:
```python
import functools

import jax
import jax.numpy as jnp
from jax import lax
from jax.experimental import pallas as pl
from jax.experimental.pallas import tpu as pltpu
from jax.sharding import PartitionSpec as P

HEAD_DIM = 64
GRID_W = 64
WIN_ROWS = 8
WIN_COLS = 16
HALO = WIN_ROWS // 2
BLOCK = 16
SHIFT = WIN_COLS // 2
STRIP = BLOCK + WIN_COLS
GROUP = 4
KEY_ROWS = GROUP + WIN_ROWS
LANES = 128
SEGMENTS = LANES // STRIP
TILES = KEY_ROWS // SEGMENTS
LOG2E = 1.4426950408889634
epsilon = 1e-06
masked_score = -1e30
F32 = jnp.float32
BF16 = jnp.bfloat16
MESH = pl.DeviceIdType.MESH


def to_peer(src, dst, send, recv, **place):
    return pltpu.make_async_remote_copy(
        src_ref=src, dst_ref=dst, send_sem=send, recv_sem=recv,
        device_id=place, device_id_type=MESH,
    )


def gcd(a, b):
    while b:
        a, b = b, a % b
    return a


def aligned(index, step):
    return pl.multiple_of(index * step, step)


def build_tables(bias_ref, braw, table, heads):
    offsets = bias_ref.shape[0]
    braw[...] = jnp.zeros_like(braw)
    for o in range(offsets):
        braw[o, :, : bias_ref.shape[2]] = bias_ref[o] * LOG2E
    lane_h = lax.broadcasted_iota(jnp.int32, (heads, LANES), 1) // STRIP
    first = HALO - 1
    combined = []
    for o in range(first - (GROUP - 1), first + (TILES - 1) * SEGMENTS + 1):
        row = braw[o]
        for j in range(1, SEGMENTS):
            row = jnp.where(lane_h == j, pltpu.roll(braw[o + j], STRIP * j, 1), row)
        combined.append(row)
    u = lax.broadcasted_iota(jnp.int32, (BLOCK, LANES), 0)
    lane = lax.broadcasted_iota(jnp.int32, (BLOCK, LANES), 1)
    v = lane % STRIP
    inner = (v >= u) & (v < u + WIN_COLS)
    edge = ((u < SHIFT) & (v < WIN_COLS)) | ((u >= SHIFT) & (v >= WIN_COLS))
    for t in range(TILES):
        for i in range(GROUP):
            j = t * SEGMENTS + lane // STRIP
            seen = (j >= i) & (j < i + WIN_ROWS)
            whole = t * SEGMENTS >= i and (t + 1) * SEGMENTS <= i + WIN_ROWS
            source = combined[t * SEGMENTS + GROUP - 1 - i]
            for h in range(heads):
                spread = jnp.broadcast_to(source[h : h + 1, :], (BLOCK, LANES))
                value = pltpu.roll(spread, LANES - (SHIFT - 1), 1, stride=1, stride_axis=0)
                place = slice((h * GROUP + i) * BLOCK, (h * GROUP + i + 1) * BLOCK)
                for kind, mask in enumerate((inner, edge)):
                    full = jnp.where(mask, value, masked_score)
                    table[kind, t, place, :] = (
                        full if whole else jnp.where(seen, full, masked_score)
                    )
                    if t != 1:
                        table[kind, 3 if t == 0 else 4, place, :] = full
    for kind in range(2):
        table[kind, 5] = jnp.full(table.shape[2:], masked_score, F32)


def kernel(
    cond_hbm, ctxcond_hbm, gain_hbm, shift_hbm, scale_hbm, gate_hbm, bias_hbm, ctx_hbm,
    lat_hbm, wq_hbm, wk_hbm, wv_hbm, wo_hbm,
    out_hbm,
    cond, ctxcond, gain, small, modw, bias, braw, table, ctx, cblk, lat, xs, wqkv, wo,
    terms, arrived, gterms, garrived, vectors, inv, q_s, kv, ctx_kv, stage, recv, obuf,
    load_sem, lat_sem, term_send, term_recv, gate_send, gate_recv, halo_send, halo_recv,
    ctx_send, ctx_recv, piece_send, piece_recv, out_sem,
):
    sp, tp = lax.axis_index("sp"), lax.axis_index("tp")
    sp_size, tp_size = lax.axis_size("sp"), lax.axis_size("tp")
    ranks = sp_size * tp_size
    me = sp * tp_size + tp
    tokens, depth = lat.shape
    width = wq_hbm.shape[1]
    heads = width // HEAD_DIM
    input_rows, piece_cols = modw.shape[1:]
    context_rows = ctx.shape[0]
    grid_rows = tokens // GRID_W
    groups = grid_rows // GROUP
    group_tokens = GROUP * GRID_W
    halo = HALO * GRID_W
    below = (HALO - 1) * GRID_W
    share = tokens // tp_size
    piece_rows = gcd(GROUP, share // GRID_W)
    piece = piece_rows * GRID_W
    pieces = share // piece
    per_group = GROUP // piece_rows

    def peer(d):
        other = (me + d) % ranks
        return dict(sp=other // tp_size, tp=other % tp_size)

    barrier = pltpu.get_barrier_semaphore()

    early = [
        pltpu.make_async_copy(cond_hbm, cond, load_sem.at[0]),
        pltpu.make_async_copy(ctxcond_hbm, ctxcond, load_sem.at[1]),
        pltpu.make_async_copy(gain_hbm, gain, load_sem.at[2]),
        pltpu.make_async_copy(shift_hbm, modw.at[0], load_sem.at[3]),
        pltpu.make_async_copy(scale_hbm, modw.at[1], load_sem.at[4]),
        pltpu.make_async_copy(gate_hbm, modw.at[2], load_sem.at[5]),
    ]
    load_bias = pltpu.make_async_copy(bias_hbm, bias, load_sem.at[6])
    load_ctx = pltpu.make_async_copy(ctx_hbm, ctx, load_sem.at[7])
    load_weights = [
        pltpu.make_async_copy(w, wqkv.at[:, pl.ds(i * width, width)], load_sem.at[8 + i])
        for i, w in enumerate((wq_hbm, wk_hbm, wv_hbm))
    ]
    load_wo = pltpu.make_async_copy(wo_hbm, wo, load_sem.at[11])

    def load_lat(i):
        rows = pl.ds(aligned(i, group_tokens), group_tokens)
        return pltpu.make_async_copy(lat_hbm.at[rows], lat.at[rows], lat_sem.at[i])

    for load in early:
        load.start()

    @pl.loop(1, ranks)
    def _(d):
        pl.semaphore_signal(barrier, inc=1, device_id=peer(d), device_id_type=MESH)

    load_bias.start()
    load_ctx.start()

    @pl.loop(0, groups)
    def _(i):
        load_lat(i).start()

    for load in load_weights:
        load.start()
    load_wo.start()

    for load in early:
        load.wait()
    small[0:1, :] = cond[...].astype(F32).reshape(1, depth)
    small[1:2, :] = ctxcond[...].astype(F32).reshape(1, depth)
    small[2:3, :] = gain[...].astype(F32).reshape(1, depth)
    row8 = lax.broadcasted_iota(jnp.int32, (8, input_rows), 0)
    own_inputs = pl.ds(aligned(sp, input_rows), input_rows)
    value = jnp.where(row8 == 0, small[0:1, own_inputs], small[1:2, own_inputs])
    act = (value / (1.0 + jnp.exp(-value))).astype(BF16)
    terms[0:2, :] = jnp.dot(act, modw[0], preferred_element_type=F32)[:2]
    terms[2:4, :] = jnp.dot(act, modw[1], preferred_element_type=F32)[:2]
    gterms[...] = jnp.dot(act, modw[2], preferred_element_type=F32)[:1]
    arrived[me] = terms[...]
    garrived[me] = gterms[...]

    def term_copy(d):
        return to_peer(terms, arrived.at[me], term_send.at[d], term_recv.at[d], **peer(d))

    def gate_copy(d):
        return to_peer(gterms, garrived.at[me], gate_send.at[d], gate_recv.at[d], **peer(d))

    load_bias.wait()
    build_tables(bias, braw, table, heads)
    pl.semaphore_wait(barrier, ranks - 1)

    @pl.loop(1, ranks)
    def _(d):
        term_copy(d).start()

    @pl.when(sp == 0)
    def _():
        kv[0:halo, :] = jnp.zeros((halo, 2 * width), BF16)

    @pl.when(sp == sp_size - 1)
    def _():
        kv[halo + tokens : halo + tokens + below, :] = jnp.zeros((below, 2 * width), BF16)

    kv[halo + tokens + below :, :] = jnp.zeros((halo - below, 2 * width), BF16)

    def inverse_of(x):
        x = x.astype(F32)
        return lax.rsqrt(jnp.mean(x * x, axis=-1, keepdims=True) + epsilon)

    load_ctx.wait()
    inv_ctx = inverse_of(ctx[...])

    @pl.loop(0, groups)
    def _(i):
        load_lat(i).wait()

        @pl.loop(0, group_tokens, step=32)
        def _(r):
            rows = pl.ds(aligned(i, group_tokens) + pl.multiple_of(r, 32), 32)
            inv[rows, :] = jnp.broadcast_to(inverse_of(lat[rows, :]), (32, LANES))

    for load in load_weights:
        load.wait()

    @pl.loop(1, ranks)
    def _(d):
        term_copy(d).wait()

    for t in range(tp_size):
        total = arrived[t]
        for s in range(1, sp_size):
            total = total + arrived[s * tp_size + t]
        vectors[:, t * piece_cols : (t + 1) * piece_cols] = total

    factor = (small[2:3, :] * (1.0 + vectors[2:3, :])).astype(BF16)
    factor_ctx = (small[2:3, :] * (1.0 + vectors[3:4, :])).astype(BF16)
    cblk[:context_rows, :] = ctx[...] * factor_ctx
    row16 = lax.broadcasted_iota(jnp.int32, (16, depth), 0)
    cblk[context_rows:, :] = jnp.where(
        row16 == 0, vectors[0:1, :], jnp.where(row16 == 1, vectors[1:2, :], 0.0)
    ).astype(BF16)
    block = jnp.dot(cblk[...], wqkv[...], preferred_element_type=F32)
    added = block[context_rows : context_rows + 1, :]
    ctx_place = pl.ds(aligned(sp, context_rows), context_rows)
    ctx_kv[ctx_place, :] = (
        block[:context_rows, width:] * inv_ctx
        + block[context_rows + 1 : context_rows + 2, width:]
    ).astype(BF16)

    def ctx_copy(d):
        return to_peer(
            ctx_kv.at[ctx_place], ctx_kv.at[ctx_place], ctx_send.at[d], ctx_recv.at[d],
            sp=(sp + d) % sp_size, tp=tp,
        )

    @pl.loop(1, sp_size)
    def _(d):
        ctx_copy(d).start()

    down = to_peer(
        kv.at[pl.ds(halo, below)], kv.at[pl.ds(halo + tokens, below)],
        halo_send.at[0], halo_recv.at[0], sp=jnp.maximum(sp - 1, 0),
    )
    up = to_peer(
        kv.at[pl.ds(tokens, halo)], kv.at[pl.ds(0, halo)],
        halo_send.at[1], halo_recv.at[1], sp=jnp.minimum(sp + 1, sp_size - 1),
    )

    @pl.loop(0, groups)
    def _(k):
        i = jnp.where(k == 0, 0, jnp.where(k == 1, groups - 1, k - 1))
        rows = pl.ds(aligned(i, group_tokens), group_tokens)
        xs[...] = lat[rows, :] * factor
        y = jnp.dot(xs[...], wqkv[...], preferred_element_type=F32)
        scale = jnp.concatenate([inv[rows, :]] * (3 * width // LANES), axis=1)
        y = y * scale + added
        q = y[:, :width] * (HEAD_DIM**-0.5 * LOG2E)
        turned = []
        for r in range(GROUP):
            turned.append(q[r * GRID_W + SHIFT : (r + 1) * GRID_W])
            turned.append(q[r * GRID_W : r * GRID_W + SHIFT])
        q_s[rows, :] = jnp.concatenate(turned, axis=0).astype(BF16)
        kv[pl.ds(aligned(i, group_tokens) + halo, group_tokens), :] = y[:, width:].astype(BF16)

        @pl.when((k == 0) & (sp > 0))
        def _():
            down.start()

        @pl.when((k == 1) & (sp < sp_size - 1))
        def _():
            up.start()

        @pl.when(k == 1)
        def _():
            @pl.loop(1, ranks)
            def _(d):
                gate_copy(d).start()

    @pl.loop(1, sp_size)
    def _(d):
        ctx_copy(d).wait()

    contract = (((1,), (1,)), ((), ()))
    stack_head = lax.broadcasted_iota(jnp.int32, (GROUP * BLOCK, width), 1) // HEAD_DIM
    blocks = GRID_W // BLOCK

    def attend(g):
        global_row = sp * grid_rows + g * GROUP
        top = global_row == 0
        bottom = global_row == sp_size * grid_rows - GROUP
        slots = (
            jnp.where(top, 5, jnp.where(bottom, 3, 0)), 1,
            jnp.where(top, 4, jnp.where(bottom, 5, 2)),
        )
        base = aligned(g, group_tokens)
        for b in range(blocks):
            kind = 1 if b == blocks - 1 else 0
            places = [
                pl.ds(base + (r * GRID_W + b * BLOCK), BLOCK) for r in range(GROUP)
            ]
            q = jnp.concatenate([q_s[place, :] for place in places], axis=0)
            stacked = jnp.concatenate(
                [jnp.where(stack_head == h, q, jnp.zeros_like(q)) for h in range(heads)], axis=0
            )
            strips = []
            for j in range(KEY_ROWS):
                if kind:
                    strips.append(pl.ds(base + (j * GRID_W + b * BLOCK), BLOCK))
                    strips.append(pl.ds(base + j * GRID_W, BLOCK))
                else:
                    strips.append(pl.ds(base + (j * GRID_W + b * BLOCK), STRIP))
            keys = jnp.concatenate([kv[s, :width] for s in strips], axis=0)
            values = jnp.concatenate([kv[s, width:] for s in strips], axis=0)
            near = lax.dot_general(stacked, keys, contract, preferred_element_type=F32)
            far = lax.dot_general(
                stacked, ctx_kv[:, :width], contract, preferred_element_type=F32
            )
            near = near + jnp.concatenate([table[kind, s] for s in slots], axis=1)
            peak = jnp.maximum(
                jnp.max(near, axis=1, keepdims=True), jnp.max(far, axis=1, keepdims=True)
            )
            near = jnp.exp2(near - peak)
            far = jnp.exp2(far - peak)
            total = jnp.sum(near, axis=1, keepdims=True) + jnp.sum(far, axis=1, keepdims=True)
            mixed = jnp.dot(
                near.astype(BF16), values, preferred_element_type=F32
            ) + jnp.dot(far.astype(BF16), ctx_kv[:, width:], preferred_element_type=F32)
            mixed = mixed * (1.0 / total)
            size = GROUP * BLOCK
            merged = mixed[:size]
            for h in range(1, heads):
                merged = jnp.where(stack_head == h, mixed[h * size : (h + 1) * size], merged)
            merged = merged.astype(BF16)
            for r, place in enumerate(places):
                stage[place, :] = merged[r * BLOCK : (r + 1) * BLOCK]

    def piece_copy(index):
        owner, p = index // pieces, index % pieces
        return to_peer(
            stage.at[pl.ds(aligned(index, piece), piece)],
            recv.at[tp, pl.ds(aligned(p, piece), piece)],
            piece_send.at[index], piece_recv.at[tp, p], tp=owner,
        )

    half = groups // 2
    upper = tp * 2 >= tp_size

    @pl.loop(0, groups)
    def _(k):
        second = k >= half
        j = jnp.where(second, k - half, k)
        low = upper != second
        g = jnp.where(low, (j + 1) % half, half + j)

        @pl.when((g == 0) & (sp > 0))
        def _():
            down.wait_send()
            up.wait_recv()

        @pl.when((g == groups - 1) & (sp < sp_size - 1))
        def _():
            up.wait_send()
            down.wait_recv()

        attend(g)
        for n in range(per_group):
            index = g * per_group + n

            @pl.when(index // pieces != tp)
            def _():
                piece_copy(index).start()

    load_wo.wait()

    @pl.loop(1, ranks)
    def _(d):
        gate_copy(d).wait()

    gates = []
    for t in range(tp_size):
        total = garrived[t]
        for s in range(1, sp_size):
            total = total + garrived[s * tp_size + t]
        gates.append(total)
    gate = jnp.concatenate(gates, axis=1)

    @pl.loop(0, pieces)
    def _(p):
        rows = pl.ds(aligned(p, piece), piece)
        own = pl.ds(aligned(tp * pieces + p, piece), piece)
        recv[tp, rows, :] = stage[own, :]

        @pl.loop(1, tp_size)
        def _(d):
            source = (tp + d) % tp_size
            to_peer(
                stage.at[own], recv.at[source, rows], piece_send.at[0],
                piece_recv.at[source, p], tp=source,
            ).wait_recv()

        mixed = jnp.concatenate([recv[t, rows, :] for t in range(tp_size)], axis=1)
        branch = jnp.dot(mixed, wo[...], preferred_element_type=F32)
        turned = []
        for r in range(piece_rows):
            turned.append(branch[(r + 1) * GRID_W - SHIFT : (r + 1) * GRID_W])
            turned.append(branch[r * GRID_W : (r + 1) * GRID_W - SHIFT])
        branch = jnp.concatenate(turned, axis=0)
        obuf[rows, :] = (lat[own, :].astype(F32) + gate * branch).astype(BF16)
        pltpu.make_async_copy(obuf.at[rows], out_hbm.at[rows], out_sem.at[p]).start()

    @pl.loop(0, pieces)
    def _(p):
        rows = pl.ds(aligned(p, piece), piece)
        pltpu.make_async_copy(obuf.at[rows], out_hbm.at[rows], out_sem.at[p]).wait()

    @pl.loop(0, groups * per_group)
    def _(index):
        @pl.when(index // pieces != tp)
        def _():
            piece_copy(index).wait_send()


def local(
    latent, condition, context_tokens, context_condition, shift_weight, scale_weight,
    gate_weight, norm_gain, query_weight, key_weight, value_weight, out_weight, offset_bias,
):
    sp_size, tp_size = lax.axis_size("sp"), lax.axis_size("tp")
    ranks = sp_size * tp_size
    tokens, depth = latent.shape
    context_rows = context_tokens.shape[0]
    input_rows, piece_cols = shift_weight.shape
    width = query_weight.shape[1]
    heads = width // HEAD_DIM
    groups = tokens // GRID_W // GROUP
    group_tokens = GROUP * GRID_W
    share = tokens // tp_size
    piece_rows = gcd(GROUP, share // GRID_W)
    pieces = share // (piece_rows * GRID_W)
    bias = jnp.transpose(offset_bias, (1, 0, 2))
    dma = pltpu.SemaphoreType.DMA
    vmem = pltpu.VMEM
    hbm = pl.BlockSpec(memory_space=pl.ANY)
    return pl.pallas_call(
        kernel,
        in_specs=[hbm] * 13,
        out_specs=hbm,
        out_shape=jax.ShapeDtypeStruct((share, depth), BF16),
        scratch_shapes=[
            vmem((depth,), BF16), vmem((depth,), BF16), vmem((depth,), BF16),
            vmem((8, depth), F32),
            vmem((3, input_rows, piece_cols), BF16),
            vmem(bias.shape, F32),
            vmem((bias.shape[0], heads, LANES), F32),
            vmem((2, 6, heads * GROUP * BLOCK, LANES), F32),
            vmem((context_rows, depth), BF16),
            vmem((context_rows + 16, depth), BF16),
            vmem((tokens, depth), BF16),
            vmem((group_tokens, depth), BF16),
            vmem((depth, 3 * width), BF16),
            vmem(out_weight.shape, BF16),
            vmem((4, piece_cols), F32),
            vmem((ranks, 4, piece_cols), F32),
            vmem((1, piece_cols), F32),
            vmem((ranks, 1, piece_cols), F32),
            vmem((4, depth), F32),
            vmem((tokens, LANES), F32),
            vmem((tokens, width), BF16),
            vmem((tokens + 2 * HALO * GRID_W, 2 * width), BF16),
            vmem((sp_size * context_rows, 2 * width), BF16),
            vmem((tokens, width), BF16),
            vmem((tp_size, share, width), BF16),
            vmem((share, depth), BF16),
            dma((12,)), dma((groups,)), dma((ranks,)), dma((ranks,)), dma((ranks,)),
            dma((ranks,)), dma((2,)), dma((2,)), dma((sp_size,)), dma((sp_size,)),
            dma((tp_size * pieces,)), dma((tp_size, pieces)), dma((pieces,)),
        ],
        compiler_params=pltpu.CompilerParams(
            vmem_limit_bytes=60 * 2**20, collective_id=0, has_side_effects=True
        ),
        cost_estimate=pl.CostEstimate(
            flops=6 * tokens * depth * width,
            bytes_accessed=2 * (tokens * depth + 3 * depth * width + share * depth),
            transcendentals=0,
        ),
    )(
        condition, context_condition, norm_gain, shift_weight, scale_weight, gate_weight, bias,
        context_tokens, latent, query_weight, key_weight, value_weight, out_weight,
    )


def solution(mesh):
    placed = (
        P(("grp", "sp"), None),
        P("grp"),
        P(("grp", "sp"), None),
        P(),
        P("sp", "tp"),
        P("sp", "tp"),
        P("sp", "tp"),
        P(),
        P(None, "tp"),
        P(None, "tp"),
        P(None, "tp"),
        P(),
        P("tp", None, None),
    )
    return jax.shard_map(
        local, mesh=mesh, in_specs=placed, out_specs=P(("grp", "sp", "tp"), None), check_vma=False
    )
```

time: 55.4 us -> 37.4 us (0.68)
  the two profiles are of different devices: /device:TPU:25 before, /device:TPU:0 now
where the time goes in v1:
time: 37.4 us; the launch traced here: 37.2 us
  Pallas kernels  34.5 us (92%)
  local copies, waits for them, and re-layouts  2.73 us (7%)
    pallas_call x1, Pallas kernels, local(): pl.pallas_call(kernel, in_specs=[hbm] * 13, out_specs=hbm, out_shape=jax....  34.5 us
    unnamed x1, local copies, waits for them, and re-layouts  2.73 us

profile of v1, /device:TPU:0, one launch (start us, length us, event | category | flops | bytes accessed | tf_op | source)
XLA Modules:
  0.0 37.2 jit_solution(9650996231481195986)
XLA Ops:
  0.0 34.5 %shard_map.127 = bf16[384,2048]{1,0:T(8,128)(2,1)} custom-call(bf16[2048]{0:T(1024)(128)(2,1)} %cond_hbm.1, bf16[2048]{0:T(1024)(128)(2,1)} %ctxcond_hbm.1, bf16[2048]{0:T(1024)(128)(2,1)} %gain_hbm.1, bf16[512,512]{1,0:T(8,128)(2,1)} %shift_hbm.1, bf16[512,512]{1,0:T(8,128)(2,1)} %scale_hbm.1, bf16[512,512]{1,0:T(8,128)(2,1)} %gate_hbm.1, ...), custom_call_target="tpu_custom_call" | custom-call | flops 4831838208 | bytes 11010048 | tf_op jit(solution)/shard_map/pallas_call | solution.py:456
  34.5 2.7 %copy.15 = bf16[384,2048]{1,0:T(8,128)(2,1)} copy(bf16[384,2048]{1,0:T(8,128)(2,1)} %shard_map.127) | data formatting | bytes 3145728

commit v2 on v1

--- a/solution.py
+++ b/solution.py
@@ -87,11 +87,12 @@
 def kernel(
     cond_hbm, ctxcond_hbm, gain_hbm, shift_hbm, scale_hbm, gate_hbm, bias_hbm, ctx_hbm,
     lat_hbm, wq_hbm, wk_hbm, wv_hbm, wo_hbm,
-    out_hbm,
+    out_ref,
     cond, ctxcond, gain, small, modw, bias, braw, table, ctx, cblk, lat, xs, wqkv, wo,
-    terms, arrived, gterms, garrived, vectors, inv, q_s, kv, ctx_kv, stage, recv, obuf,
-    load_sem, lat_sem, term_send, term_recv, gate_send, gate_recv, halo_send, halo_recv,
-    ctx_send, ctx_recv, piece_send, piece_recv, out_sem,
+    cterms, carrived, terms, arrived, gterms, garrived, vectors, inv, q_s, kv, ctx_kv,
+    scores, probs, stage, recv, acc,
+    load_sem, lat_sem, cterm_send, cterm_recv, term_send, term_recv, gate_send, gate_recv,
+    halo_send, halo_recv, ctx_send, ctx_recv, piece_send, piece_recv,
 ):
     sp, tp = lax.axis_index("sp"), lax.axis_index("tp")
     sp_size, tp_size = lax.axis_size("sp"), lax.axis_size("tp")
@@ -112,6 +113,8 @@
     piece = piece_rows * GRID_W
     pieces = share // piece
     per_group = GROUP // piece_rows
+    big = xs.shape[0] - 16
+    steps = tokens // big
 
     def peer(d):
         other = (me + d) % ranks
@@ -139,12 +142,12 @@
         rows = pl.ds(aligned(i, group_tokens), group_tokens)
         return pltpu.make_async_copy(lat_hbm.at[rows], lat.at[rows], lat_sem.at[i])
 
+    @pl.loop(1, ranks)
+    def _(d):
+        pl.semaphore_signal(barrier, inc=1, device_id=peer(d), device_id_type=MESH)
+
     for load in early:
         load.start()
-
-    @pl.loop(1, ranks)
-    def _(d):
-        pl.semaphore_signal(barrier, inc=1, device_id=peer(d), device_id_type=MESH)
 
     load_bias.start()
     load_ctx.start()
@@ -166,11 +169,19 @@
     own_inputs = pl.ds(aligned(sp, input_rows), input_rows)
     value = jnp.where(row8 == 0, small[0:1, own_inputs], small[1:2, own_inputs])
     act = (value / (1.0 + jnp.exp(-value))).astype(BF16)
-    terms[0:2, :] = jnp.dot(act, modw[0], preferred_element_type=F32)[:2]
-    terms[2:4, :] = jnp.dot(act, modw[1], preferred_element_type=F32)[:2]
+    for i in range(2):
+        both = jnp.dot(act, modw[i], preferred_element_type=F32)
+        terms[i : i + 1, :] = both[0:1]
+        cterms[i : i + 1, :] = both[1:2]
     gterms[...] = jnp.dot(act, modw[2], preferred_element_type=F32)[:1]
+    carrived[me] = cterms[...]
     arrived[me] = terms[...]
     garrived[me] = gterms[...]
+
+    def cterm_copy(d):
+        return to_peer(
+            cterms, carrived.at[me], cterm_send.at[d], cterm_recv.at[d], **peer(d)
+        )
 
     def term_copy(d):
         return to_peer(terms, arrived.at[me], term_send.at[d], term_recv.at[d], **peer(d))
@@ -184,6 +195,10 @@
 
     @pl.loop(1, ranks)
     def _(d):
+        cterm_copy(d).start()
+
+    @pl.loop(1, ranks)
+    def _(d):
         term_copy(d).start()
 
     @pl.when(sp == 0)
@@ -196,48 +211,47 @@
 
     kv[halo + tokens + below :, :] = jnp.zeros((halo - below, 2 * width), BF16)
 
-    def inverse_of(x):
-        x = x.astype(F32)
-        return lax.rsqrt(jnp.mean(x * x, axis=-1, keepdims=True) + epsilon)
+    def inverse_of(ref, rows):
+        total = None
+        for c in range(depth // LANES):
+            x = ref[rows, c * LANES : (c + 1) * LANES].astype(F32)
+            total = x * x if total is None else total + x * x
+        mean = jnp.sum(total, axis=1, keepdims=True) * (1.0 / depth)
+        return lax.rsqrt(mean + epsilon)
 
     load_ctx.wait()
-    inv_ctx = inverse_of(ctx[...])
+    inv_ctx = inverse_of(ctx, slice(None))
 
     @pl.loop(0, groups)
     def _(i):
         load_lat(i).wait()
-
-        @pl.loop(0, group_tokens, step=32)
-        def _(r):
-            rows = pl.ds(aligned(i, group_tokens) + pl.multiple_of(r, 32), 32)
-            inv[rows, :] = jnp.broadcast_to(inverse_of(lat[rows, :]), (32, LANES))
+        for r in range(0, group_tokens, 128):
+            rows = pl.ds(aligned(i, group_tokens) + r, 128)
+            inv[rows, :] = jnp.broadcast_to(inverse_of(lat, rows), (128, LANES))
 
     for load in load_weights:
         load.wait()
 
+    def sum_terms(ref, rows):
+        for t in range(tp_size):
+            total = ref[t]
+            for s in range(1, sp_size):
+                total = total + ref[s * tp_size + t]
+            vectors[rows, t * piece_cols : (t + 1) * piece_cols] = total
+
     @pl.loop(1, ranks)
     def _(d):
-        term_copy(d).wait()
-
-    for t in range(tp_size):
-        total = arrived[t]
-        for s in range(1, sp_size):
-            total = total + arrived[s * tp_size + t]
-        vectors[:, t * piece_cols : (t + 1) * piece_cols] = total
-
-    factor = (small[2:3, :] * (1.0 + vectors[2:3, :])).astype(BF16)
-    factor_ctx = (small[2:3, :] * (1.0 + vectors[3:4, :])).astype(BF16)
+        cterm_copy(d).wait()
+
+    sum_terms(carrived, slice(0, 2))
+    row16 = lax.broadcasted_iota(jnp.int32, (16, depth), 0)
+    factor_ctx = (small[2:3, :] * (1.0 + vectors[1:2, :])).astype(BF16)
     cblk[:context_rows, :] = ctx[...] * factor_ctx
-    row16 = lax.broadcasted_iota(jnp.int32, (16, depth), 0)
-    cblk[context_rows:, :] = jnp.where(
-        row16 == 0, vectors[0:1, :], jnp.where(row16 == 1, vectors[1:2, :], 0.0)
-    ).astype(BF16)
-    block = jnp.dot(cblk[...], wqkv[...], preferred_element_type=F32)
-    added = block[context_rows : context_rows + 1, :]
+    cblk[context_rows:, :] = jnp.where(row16 == 0, vectors[0:1, :], 0.0).astype(BF16)
+    block = jnp.dot(cblk[...], wqkv[:, width:], preferred_element_type=F32)
     ctx_place = pl.ds(aligned(sp, context_rows), context_rows)
     ctx_kv[ctx_place, :] = (
-        block[:context_rows, width:] * inv_ctx
-        + block[context_rows + 1 : context_rows + 2, width:]
+        block[:context_rows] * inv_ctx + block[context_rows : context_rows + 1]
     ).astype(BF16)
 
     def ctx_copy(d):
@@ -259,31 +273,39 @@
         halo_send.at[1], halo_recv.at[1], sp=jnp.minimum(sp + 1, sp_size - 1),
     )
 
-    @pl.loop(0, groups)
+    @pl.loop(1, ranks)
+    def _(d):
+        term_copy(d).wait()
+
+    sum_terms(arrived, slice(2, 4))
+    factor = (small[2:3, :] * (1.0 + vectors[3:4, :])).astype(BF16)
+    xs[big:, :] = jnp.where(row16 == 0, vectors[2:3, :], 0.0).astype(BF16)
+
+    @pl.loop(0, steps)
     def _(k):
-        i = jnp.where(k == 0, 0, jnp.where(k == 1, groups - 1, k - 1))
-        rows = pl.ds(aligned(i, group_tokens), group_tokens)
-        xs[...] = lat[rows, :] * factor
+        i = jnp.where(k == 0, 0, jnp.where(k == 1, steps - 1, k - 1))
+        rows = pl.ds(aligned(i, big), big)
+        xs[:big, :] = lat[rows, :] * factor
         y = jnp.dot(xs[...], wqkv[...], preferred_element_type=F32)
         scale = jnp.concatenate([inv[rows, :]] * (3 * width // LANES), axis=1)
-        y = y * scale + added
+        y = y[:big] * scale + y[big : big + 1]
         q = y[:, :width] * (HEAD_DIM**-0.5 * LOG2E)
         turned = []
-        for r in range(GROUP):
+        for r in range(big // GRID_W):
             turned.append(q[r * GRID_W + SHIFT : (r + 1) * GRID_W])
             turned.append(q[r * GRID_W : r * GRID_W + SHIFT])
         q_s[rows, :] = jnp.concatenate(turned, axis=0).astype(BF16)
-        kv[pl.ds(aligned(i, group_tokens) + halo, group_tokens), :] = y[:, width:].astype(BF16)
+        kv[pl.ds(aligned(i, big) + halo, big), :] = y[:, width:].astype(BF16)
 
         @pl.when((k == 0) & (sp > 0))
         def _():
             down.start()
 
-        @pl.when((k == 1) & (sp < sp_size - 1))
+        @pl.when((k == min(1, steps - 1)) & (sp < sp_size - 1))
         def _():
             up.start()
 
-        @pl.when(k == 1)
+        @pl.when(k == min(1, steps - 1))
         def _():
             @pl.loop(1, ranks)
             def _(d):
@@ -294,8 +316,11 @@
         ctx_copy(d).wait()
 
     contract = (((1,), (1,)), ((), ()))
-    stack_head = lax.broadcasted_iota(jnp.int32, (GROUP * BLOCK, width), 1) // HEAD_DIM
+    size = GROUP * BLOCK
+    stack_head = lax.broadcasted_iota(jnp.int32, (size, width), 1) // HEAD_DIM
+    first_head = lax.broadcasted_iota(jnp.int32, (size, LANES), 1) < HEAD_DIM
     blocks = GRID_W // BLOCK
+    near_keys = KEY_ROWS * STRIP
 
     def attend(g):
         global_row = sp * grid_rows + g * GROUP
@@ -306,46 +331,69 @@
             jnp.where(top, 4, jnp.where(bottom, 5, 2)),
         )
         base = aligned(g, group_tokens)
-        for b in range(blocks):
+
+        def strips(b):
+            found = []
+            for j in range(KEY_ROWS):
+                if b == blocks - 1:
+                    found.append(pl.ds(base + (j * GRID_W + b * BLOCK), BLOCK))
+                    found.append(pl.ds(base + j * GRID_W, BLOCK))
+                else:
+                    found.append(pl.ds(base + (j * GRID_W + b * BLOCK), STRIP))
+            return found
+
+        def places(b):
+            return [pl.ds(base + (r * GRID_W + b * BLOCK), BLOCK) for r in range(GROUP)]
+
+        def score(b):
             kind = 1 if b == blocks - 1 else 0
-            places = [
-                pl.ds(base + (r * GRID_W + b * BLOCK), BLOCK) for r in range(GROUP)
-            ]
-            q = jnp.concatenate([q_s[place, :] for place in places], axis=0)
+            q = jnp.concatenate([q_s[place, :] for place in places(b)], axis=0)
             stacked = jnp.concatenate(
                 [jnp.where(stack_head == h, q, jnp.zeros_like(q)) for h in range(heads)], axis=0
             )
-            strips = []
-            for j in range(KEY_ROWS):
-                if kind:
-                    strips.append(pl.ds(base + (j * GRID_W + b * BLOCK), BLOCK))
-                    strips.append(pl.ds(base + j * GRID_W, BLOCK))
-                else:
-                    strips.append(pl.ds(base + (j * GRID_W + b * BLOCK), STRIP))
-            keys = jnp.concatenate([kv[s, :width] for s in strips], axis=0)
-            values = jnp.concatenate([kv[s, width:] for s in strips], axis=0)
-            near = lax.dot_general(stacked, keys, contract, preferred_element_type=F32)
-            far = lax.dot_general(
-                stacked, ctx_kv[:, :width], contract, preferred_element_type=F32
+            keys = jnp.concatenate(
+                [kv[s, :width] for s in strips(b)] + [ctx_kv[:, :width]], axis=0
             )
-            near = near + jnp.concatenate([table[kind, s] for s in slots], axis=1)
-            peak = jnp.maximum(
-                jnp.max(near, axis=1, keepdims=True), jnp.max(far, axis=1, keepdims=True)
+            s = lax.dot_general(stacked, keys, contract, preferred_element_type=F32)
+            for t in range(TILES):
+                lanes = slice(t * LANES, (t + 1) * LANES)
+                scores[b, :, lanes] = s[:, lanes] + table[kind, slots[t]]
+            scores[b, :, near_keys:] = s[:, near_keys:]
+
+        def soften(b):
+            sums = []
+            for h in range(heads):
+                rows = slice(h * size, (h + 1) * size)
+                s = scores[b, rows, :]
+                p = jnp.exp2(s - jnp.max(s, axis=1, keepdims=True))
+                sums.append(jnp.sum(p, axis=1, keepdims=True))
+                probs[b, rows, :] = p.astype(BF16)
+            return [1.0 / total for total in sums]
+
+        def mix(b, inverses):
+            values = jnp.concatenate(
+                [kv[s, width:] for s in strips(b)] + [ctx_kv[:, width:]], axis=0
             )
-            near = jnp.exp2(near - peak)
-            far = jnp.exp2(far - peak)
-            total = jnp.sum(near, axis=1, keepdims=True) + jnp.sum(far, axis=1, keepdims=True)
-            mixed = jnp.dot(
-                near.astype(BF16), values, preferred_element_type=F32
-            ) + jnp.dot(far.astype(BF16), ctx_kv[:, width:], preferred_element_type=F32)
-            mixed = mixed * (1.0 / total)
-            size = GROUP * BLOCK
-            merged = mixed[:size]
-            for h in range(1, heads):
-                merged = jnp.where(stack_head == h, mixed[h * size : (h + 1) * size], merged)
-            merged = merged.astype(BF16)
-            for r, place in enumerate(places):
+            mixed = jnp.dot(probs[b], values, preferred_element_type=F32)
+            parts = []
+            for c in range(width // LANES):
+                h, lanes = 2 * c, slice(c * LANES, (c + 1) * LANES)
+                parts.append(
+                    jnp.where(
+                        first_head,
+                        mixed[h * size : (h + 1) * size, lanes] * inverses[h],
+                        mixed[(h + 1) * size : (h + 2) * size, lanes] * inverses[h + 1],
+                    )
+                )
+            merged = jnp.concatenate(parts, axis=1).astype(BF16)
+            for r, place in enumerate(places(b)):
                 stage[place, :] = merged[r * BLOCK : (r + 1) * BLOCK]
+
+        score(0)
+        for b in range(blocks):
+            if b + 1 < blocks:
+                score(b + 1)
+            mix(b, soften(b))
 
     def piece_copy(index):
         owner, p = index // pieces, index % pieces
@@ -396,35 +444,47 @@
             total = total + garrived[s * tp_size + t]
         gates.append(total)
     gate = jnp.concatenate(gates, axis=1)
+    chips = tp_size // 2
+    chip = tp // 2
+    partner = tp + 1 - 2 * (tp % 2)
+
+    def arrival(source, p):
+        rows = pl.ds(aligned(p, piece), piece)
+        return to_peer(
+            stage.at[rows], recv.at[source, rows], piece_send.at[0],
+            piece_recv.at[source, p], tp=source,
+        )
+
+    def product(c, rows):
+        pair = jnp.concatenate([recv[2 * c, rows, :], recv[2 * c + 1, rows, :]], axis=1)
+        return jnp.dot(
+            pair, wo[pl.ds(aligned(c, 2 * width), 2 * width), :], preferred_element_type=F32
+        )
 
     @pl.loop(0, pieces)
     def _(p):
         rows = pl.ds(aligned(p, piece), piece)
+        recv[tp, rows, :] = stage[pl.ds(aligned(tp * pieces + p, piece), piece), :]
+        arrival(partner, p).wait_recv()
+        acc[rows, :] = product(chip, rows)
+
+    @pl.loop(0, pieces)
+    def _(k):
+        p = jnp.where(tp == 0, (k + per_group) % pieces, k)
+        rows = pl.ds(aligned(p, piece), piece)
         own = pl.ds(aligned(tp * pieces + p, piece), piece)
-        recv[tp, rows, :] = stage[own, :]
-
-        @pl.loop(1, tp_size)
-        def _(d):
-            source = (tp + d) % tp_size
-            to_peer(
-                stage.at[own], recv.at[source, rows], piece_send.at[0],
-                piece_recv.at[source, p], tp=source,
-            ).wait_recv()
-
-        mixed = jnp.concatenate([recv[t, rows, :] for t in range(tp_size)], axis=1)
-        branch = jnp.dot(mixed, wo[...], preferred_element_type=F32)
+        branch = acc[rows, :]
+        for d in range(1, chips):
+            c = (chip + d) % chips
+            arrival(2 * c, p).wait_recv()
+            arrival(2 * c + 1, p).wait_recv()
+            branch = branch + product(c, rows)
         turned = []
         for r in range(piece_rows):
             turned.append(branch[(r + 1) * GRID_W - SHIFT : (r + 1) * GRID_W])
             turned.append(branch[r * GRID_W : (r + 1) * GRID_W - SHIFT])
         branch = jnp.concatenate(turned, axis=0)
-        obuf[rows, :] = (lat[own, :].astype(F32) + gate * branch).astype(BF16)
-        pltpu.make_async_copy(obuf.at[rows], out_hbm.at[rows], out_sem.at[p]).start()
-
-    @pl.loop(0, pieces)
-    def _(p):
-        rows = pl.ds(aligned(p, piece), piece)
-        pltpu.make_async_copy(obuf.at[rows], out_hbm.at[rows], out_sem.at[p]).wait()
+        out_ref[rows, :] = (lat[own, :].astype(F32) + gate * branch).astype(BF16)
 
     @pl.loop(0, groups * per_group)
     def _(index):
@@ -449,6 +509,9 @@
     share = tokens // tp_size
     piece_rows = gcd(GROUP, share // GRID_W)
     pieces = share // (piece_rows * GRID_W)
+    big = 2 * group_tokens if groups % 2 == 0 else group_tokens
+    stacked = heads * GROUP * BLOCK
+    keys = KEY_ROWS * STRIP + sp_size * context_rows
     bias = jnp.transpose(offset_bias, (1, 0, 2))
     dma = pltpu.SemaphoreType.DMA
     vmem = pltpu.VMEM
@@ -456,8 +519,8 @@
     return pl.pallas_call(
         kernel,
         in_specs=[hbm] * 13,
-        out_specs=hbm,
-        out_shape=jax.ShapeDtypeStruct((share, depth), BF16),
+        out_specs=pl.BlockSpec(memory_space=pltpu.VMEM),
+        out_shape=pltpu.VMEM((share, depth), BF16),
         scratch_shapes=[
             vmem((depth,), BF16), vmem((depth,), BF16), vmem((depth,), BF16),
             vmem((8, depth), F32),
@@ -468,11 +531,13 @@
             vmem((context_rows, depth), BF16),
             vmem((context_rows + 16, depth), BF16),
             vmem((tokens, depth), BF16),
-            vmem((group_tokens, depth), BF16),
+            vmem((big + 16, depth), BF16),
             vmem((depth, 3 * width), BF16),
             vmem(out_weight.shape, BF16),
-            vmem((4, piece_cols), F32),
-            vmem((ranks, 4, piece_cols), F32),
+            vmem((2, piece_cols), F32),
+            vmem((ranks, 2, piece_cols), F32),
+            vmem((2, piece_cols), F32),
+            vmem((ranks, 2, piece_cols), F32),
             vmem((1, piece_cols), F32),
             vmem((ranks, 1, piece_cols), F32),
             vmem((4, depth), F32),
@@ -480,12 +545,15 @@
             vmem((tokens, width), BF16),
             vmem((tokens + 2 * HALO * GRID_W, 2 * width), BF16),
             vmem((sp_size * context_rows, 2 * width), BF16),
+            vmem((GRID_W // BLOCK, stacked, keys), F32),
+            vmem((GRID_W // BLOCK, stacked, keys), BF16),
             vmem((tokens, width), BF16),
             vmem((tp_size, share, width), BF16),
-            vmem((share, depth), BF16),
+            vmem((share, depth), F32),
             dma((12,)), dma((groups,)), dma((ranks,)), dma((ranks,)), dma((ranks,)),
-            dma((ranks,)), dma((2,)), dma((2,)), dma((sp_size,)), dma((sp_size,)),
-            dma((tp_size * pieces,)), dma((tp_size, pieces)), dma((pieces,)),
+            dma((ranks,)), dma((ranks,)), dma((ranks,)), dma((2,)), dma((2,)),
+            dma((sp_size,)), dma((sp_size,)),
+            dma((tp_size * pieces,)), dma((tp_size, pieces)),
         ],
         compiler_params=pltpu.CompilerParams(
             vmem_limit_bytes=60 * 2**20, collective_id=0, has_side_effects=True

time: 37.4 us -> 33.8 us (0.904)
  the two profiles are of different devices: /device:TPU:0 before, /device:TPU:19 now
where the time goes in v2:
time: 33.8 us; the launch traced here: 33.6 us
  Pallas kernels  32.4 us (96%)
  local copies, waits for them, and re-layouts  1.15 us (3%)
    pallas_call x1, Pallas kernels, local(): pl.pallas_call(kernel, in_specs=[hbm] * 13, out_specs=pl.BlockSpec(memory...  32.4 us
    unnamed x1, local copies, waits for them, and re-layouts  1.15 us

profile of v2, /device:TPU:19, one launch (start us, length us, event | category | flops | bytes accessed | tf_op | source)
XLA Modules:
  0.0 33.6 jit_solution(1354109630411633699)
XLA Ops:
  0.0 32.4 %shard_map.127 = bf16[384,2048]{1,0:T(8,128)(2,1)S(1)} custom-call(bf16[2048]{0:T(1024)(128)(2,1)} %cond_hbm.1, bf16[2048]{0:T(1024)(128)(2,1)} %ctxcond_hbm.1, bf16[2048]{0:T(1024)(128)(2,1)} %gain_hbm.1, bf16[512,512]{1,0:T(8,128)(2,1)} %shift_hbm.1, bf16[512,512]{1,0:T(8,128)(2,1)} %scale_hbm.1, bf16[512,512]{1,0:T(8,128)(2,1)} %gate_hbm.1, ...), custom_call_target="tpu_custom_call" | custom-call | flops 4831838208 | bytes 11010048 | tf_op jit(solution)/shard_map/pallas_call | solution.py:519
  32.4 1.1 %copy.15 = bf16[384,2048]{1,0:T(8,128)(2,1)} copy(bf16[384,2048]{1,0:T(8,128)(2,1)S(1)} %shard_map.127) | data formatting | bytes 3145728

commit v3 on v2

--- a/solution.py
+++ b/solution.py
@@ -89,7 +89,7 @@
     lat_hbm, wq_hbm, wk_hbm, wv_hbm, wo_hbm,
     out_ref,
     cond, ctxcond, gain, small, modw, bias, braw, table, ctx, cblk, lat, xs, wqkv, wo,
-    cterms, carrived, terms, arrived, gterms, garrived, vectors, inv, q_s, kv, ctx_kv,
+    cterms, carrived, terms, arrived, gterms, garrived, vectors, added, inv, q_s, kv, ctx_kv,
     scores, probs, stage, recv, acc,
     load_sem, lat_sem, cterm_send, cterm_recv, term_send, term_recv, gate_send, gate_recv,
     halo_send, halo_recv, ctx_send, ctx_recv, piece_send, piece_recv,
@@ -113,8 +113,6 @@
     piece = piece_rows * GRID_W
     pieces = share // piece
     per_group = GROUP // piece_rows
-    big = xs.shape[0] - 16
-    steps = tokens // big
 
     def peer(d):
         other = (me + d) % ranks
@@ -279,41 +277,57 @@
 
     sum_terms(arrived, slice(2, 4))
     factor = (small[2:3, :] * (1.0 + vectors[3:4, :])).astype(BF16)
-    xs[big:, :] = jnp.where(row16 == 0, vectors[2:3, :], 0.0).astype(BF16)
-
-    @pl.loop(0, steps)
-    def _(k):
-        i = jnp.where(k == 0, 0, jnp.where(k == 1, steps - 1, k - 1))
-        rows = pl.ds(aligned(i, big), big)
-        xs[:big, :] = lat[rows, :] * factor
-        y = jnp.dot(xs[...], wqkv[...], preferred_element_type=F32)
-        scale = jnp.concatenate([inv[rows, :]] * (3 * width // LANES), axis=1)
-        y = y[:big] * scale + y[big : big + 1]
-        q = y[:, :width] * (HEAD_DIM**-0.5 * LOG2E)
+    xs[group_tokens:, :] = jnp.where(row16 == 0, vectors[2:3, :], 0.0).astype(BF16)
+
+    upper = tp * 2 >= tp_size
+
+    def unit(k):
+        if k == 0:
+            return jnp.where(upper, groups - 1, 0)
+        if k == groups - 1:
+            return jnp.where(upper, groups - 2, 1)
+        return jnp.where(upper, k - 1, k + 1)
+
+    def project(i, first):
+        rows = pl.ds(aligned(i, group_tokens), group_tokens)
+        place = pl.ds(aligned(i, group_tokens) + halo, group_tokens)
+        xs[:group_tokens, :] = lat[rows, :] * factor
+        scale = jnp.concatenate([inv[rows, :]] * (width // LANES), axis=1)
+
+        def part(n):
+            columns = slice(n * width, (n + 1) * width)
+            left = xs[...] if first else xs[:group_tokens, :]
+            y = jnp.dot(left, wqkv[:, columns], preferred_element_type=F32)
+            if first:
+                added[0:1, columns] = y[group_tokens : group_tokens + 1]
+            return y[:group_tokens] * scale + added[0:1, columns]
+
+        q = part(0) * (HEAD_DIM**-0.5 * LOG2E)
         turned = []
-        for r in range(big // GRID_W):
+        for r in range(GROUP):
             turned.append(q[r * GRID_W + SHIFT : (r + 1) * GRID_W])
             turned.append(q[r * GRID_W : r * GRID_W + SHIFT])
         q_s[rows, :] = jnp.concatenate(turned, axis=0).astype(BF16)
-        kv[pl.ds(aligned(i, big) + halo, big), :] = y[:, width:].astype(BF16)
-
-        @pl.when((k == 0) & (sp > 0))
+        kv[place, :width] = part(1).astype(BF16)
+        kv[place, width:] = part(2).astype(BF16)
+
+    project(unit(0), True)
+
+    @pl.loop(1, groups - 1)
+    def _(k):
+        project(jnp.where(upper, k - 1, k + 1), False)
+
+        @pl.when((k == 1) & (sp > 0))
         def _():
             down.start()
 
-        @pl.when((k == min(1, steps - 1)) & (sp < sp_size - 1))
+        @pl.when((k == groups - 2) & (sp < sp_size - 1))
         def _():
             up.start()
 
-        @pl.when(k == min(1, steps - 1))
-        def _():
-            @pl.loop(1, ranks)
-            def _(d):
-                gate_copy(d).start()
-
-    @pl.loop(1, sp_size)
-    def _(d):
-        ctx_copy(d).wait()
+    @pl.loop(1, ranks)
+    def _(d):
+        gate_copy(d).start()
 
     contract = (((1,), (1,)), ((), ()))
     size = GROUP * BLOCK
@@ -322,7 +336,28 @@
     blocks = GRID_W // BLOCK
     near_keys = KEY_ROWS * STRIP
 
-    def attend(g):
+    def strips(g, b):
+        base = aligned(g, group_tokens)
+        found = []
+        for j in range(KEY_ROWS):
+            if b == blocks - 1:
+                found.append(pl.ds(base + (j * GRID_W + b * BLOCK), BLOCK))
+                found.append(pl.ds(base + j * GRID_W, BLOCK))
+            else:
+                found.append(pl.ds(base + (j * GRID_W + b * BLOCK), STRIP))
+        return found
+
+    def places(g, b):
+        base = aligned(g, group_tokens)
+        return [pl.ds(base + (r * GRID_W + b * BLOCK), BLOCK) for r in range(GROUP)]
+
+    def stacked(g, b):
+        q = jnp.concatenate([q_s[place, :] for place in places(g, b)], axis=0)
+        return jnp.concatenate(
+            [jnp.where(stack_head == h, q, jnp.zeros_like(q)) for h in range(heads)], axis=0
+        )
+
+    def score_near(g, b):
         global_row = sp * grid_rows + g * GROUP
         top = global_row == 0
         bottom = global_row == sp_size * grid_rows - GROUP
@@ -330,70 +365,46 @@
             jnp.where(top, 5, jnp.where(bottom, 3, 0)), 1,
             jnp.where(top, 4, jnp.where(bottom, 5, 2)),
         )
-        base = aligned(g, group_tokens)
-
-        def strips(b):
-            found = []
-            for j in range(KEY_ROWS):
-                if b == blocks - 1:
-                    found.append(pl.ds(base + (j * GRID_W + b * BLOCK), BLOCK))
-                    found.append(pl.ds(base + j * GRID_W, BLOCK))
-                else:
-                    found.append(pl.ds(base + (j * GRID_W + b * BLOCK), STRIP))
-            return found
-
-        def places(b):
-            return [pl.ds(base + (r * GRID_W + b * BLOCK), BLOCK) for r in range(GROUP)]
-
-        def score(b):
-            kind = 1 if b == blocks - 1 else 0
-            q = jnp.concatenate([q_s[place, :] for place in places(b)], axis=0)
-            stacked = jnp.concatenate(
-                [jnp.where(stack_head == h, q, jnp.zeros_like(q)) for h in range(heads)], axis=0
+        kind = 1 if b == blocks - 1 else 0
+        keys = jnp.concatenate([kv[s, :width] for s in strips(g, b)], axis=0)
+        s = lax.dot_general(stacked(g, b), keys, contract, preferred_element_type=F32)
+        for t in range(TILES):
+            lanes = slice(t * LANES, (t + 1) * LANES)
+            scores[b, :, lanes] = s[:, lanes] + table[kind, slots[t]]
+
+    def score_far(g, b):
+        scores[b, :, near_keys:] = lax.dot_general(
+            stacked(g, b), ctx_kv[:, :width], contract, preferred_element_type=F32
+        )
+
+    def soften(b):
+        sums = []
+        for h in range(heads):
+            rows = slice(h * size, (h + 1) * size)
+            s = scores[b, rows, :]
+            p = jnp.exp2(s - jnp.max(s, axis=1, keepdims=True))
+            sums.append(jnp.sum(p, axis=1, keepdims=True))
+            probs[b, rows, :] = p.astype(BF16)
+        return [1.0 / total for total in sums]
+
+    def mix(g, b, inverses):
+        values = jnp.concatenate(
+            [kv[s, width:] for s in strips(g, b)] + [ctx_kv[:, width:]], axis=0
+        )
+        mixed = jnp.dot(probs[b], values, preferred_element_type=F32)
+        parts = []
+        for c in range(width // LANES):
+            h, lanes = 2 * c, slice(c * LANES, (c + 1) * LANES)
+            parts.append(
+                jnp.where(
+                    first_head,
+                    mixed[h * size : (h + 1) * size, lanes] * inverses[h],
+                    mixed[(h + 1) * size : (h + 2) * size, lanes] * inverses[h + 1],
+                )
             )
-            keys = jnp.concatenate(
-                [kv[s, :width] for s in strips(b)] + [ctx_kv[:, :width]], axis=0
-            )
-            s = lax.dot_general(stacked, keys, contract, preferred_element_type=F32)
-            for t in range(TILES):
-                lanes = slice(t * LANES, (t + 1) * LANES)
-                scores[b, :, lanes] = s[:, lanes] + table[kind, slots[t]]
-            scores[b, :, near_keys:] = s[:, near_keys:]
-
-        def soften(b):
-            sums = []
-            for h in range(heads):
-                rows = slice(h * size, (h + 1) * size)
-                s = scores[b, rows, :]
-                p = jnp.exp2(s - jnp.max(s, axis=1, keepdims=True))
-                sums.append(jnp.sum(p, axis=1, keepdims=True))
-                probs[b, rows, :] = p.astype(BF16)
-            return [1.0 / total for total in sums]
-
-        def mix(b, inverses):
-            values = jnp.concatenate(
-                [kv[s, width:] for s in strips(b)] + [ctx_kv[:, width:]], axis=0
-            )
-            mixed = jnp.dot(probs[b], values, preferred_element_type=F32)
-            parts = []
-            for c in range(width // LANES):
-                h, lanes = 2 * c, slice(c * LANES, (c + 1) * LANES)
-                parts.append(
-                    jnp.where(
-                        first_head,
-                        mixed[h * size : (h + 1) * size, lanes] * inverses[h],
-                        mixed[(h + 1) * size : (h + 2) * size, lanes] * inverses[h + 1],
-                    )
-                )
-            merged = jnp.concatenate(parts, axis=1).astype(BF16)
-            for r, place in enumerate(places(b)):
-                stage[place, :] = merged[r * BLOCK : (r + 1) * BLOCK]
-
-        score(0)
-        for b in range(blocks):
-            if b + 1 < blocks:
-                score(b + 1)
-            mix(b, soften(b))
+        merged = jnp.concatenate(parts, axis=1).astype(BF16)
+        for r, place in enumerate(places(g, b)):
+            stage[place, :] = merged[r * BLOCK : (r + 1) * BLOCK]
 
     def piece_copy(index):
         owner, p = index // pieces, index % pieces
@@ -404,14 +415,46 @@
         )
 
     half = groups // 2
-    upper = tp * 2 >= tp_size
-
-    @pl.loop(0, groups)
+    inner = half - 1
+
+    def group_of(own, j):
+        return jnp.where(upper != own, (j + 1) % half, half + j)
+
+    def send_pieces(g):
+        for n in range(per_group):
+            index = g * per_group + n
+
+            @pl.when(index // pieces != tp)
+            def _():
+                piece_copy(index).start()
+
+    for b in range(blocks):
+        score_near(group_of(False, 0), b)
+
+    @pl.loop(1, sp_size)
+    def _(d):
+        ctx_copy(d).wait()
+
+    @pl.loop(0, inner)
     def _(k):
-        second = k >= half
-        j = jnp.where(second, k - half, k)
-        low = upper != second
-        g = jnp.where(low, (j + 1) % half, half + j)
+        g, following = group_of(False, k), group_of(False, jnp.minimum(k + 1, inner - 1))
+        score_far(g, 0)
+        for b in range(blocks):
+            if b + 1 < blocks:
+                score_far(g, b + 1)
+            inverses = soften(b)
+            score_near(following, b)
+            mix(g, b, inverses)
+        send_pieces(g)
+
+    project(unit(groups - 1), False)
+
+    @pl.loop(0, groups - inner)
+    def _(k):
+        edge = (k == 1) | (k == groups - inner - 1)
+        own = k != 1
+        j = jnp.where(edge, inner, jnp.where(k > 1, k - 1, k))
+        g = group_of(own, j)
 
         @pl.when((g == 0) & (sp > 0))
         def _():
@@ -423,13 +466,14 @@
             up.wait_send()
             down.wait_recv()
 
-        attend(g)
-        for n in range(per_group):
-            index = g * per_group + n
-
-            @pl.when(index // pieces != tp)
-            def _():
-                piece_copy(index).start()
+        score_near(g, 0)
+        score_far(g, 0)
+        for b in range(blocks):
+            if b + 1 < blocks:
+                score_near(g, b + 1)
+                score_far(g, b + 1)
+            mix(g, b, soften(b))
+        send_pieces(g)
 
     load_wo.wait()
 
@@ -467,6 +511,12 @@
         recv[tp, rows, :] = stage[pl.ds(aligned(tp * pieces + p, piece), piece), :]
         arrival(partner, p).wait_recv()
         acc[rows, :] = product(chip, rows)
+
+    @pl.loop(0, groups * per_group)
+    def _(index):
+        @pl.when(index // pieces != tp)
+        def _():
+            piece_copy(index).wait_send()
 
     @pl.loop(0, pieces)
     def _(k):
@@ -486,12 +536,6 @@
         branch = jnp.concatenate(turned, axis=0)
         out_ref[rows, :] = (lat[own, :].astype(F32) + gate * branch).astype(BF16)
 
-    @pl.loop(0, groups * per_group)
-    def _(index):
-        @pl.when(index // pieces != tp)
-        def _():
-            piece_copy(index).wait_send()
-
 
 def local(
     latent, condition, context_tokens, context_condition, shift_weight, scale_weight,
@@ -509,7 +553,6 @@
     share = tokens // tp_size
     piece_rows = gcd(GROUP, share // GRID_W)
     pieces = share // (piece_rows * GRID_W)
-    big = 2 * group_tokens if groups % 2 == 0 else group_tokens
     stacked = heads * GROUP * BLOCK
     keys = KEY_ROWS * STRIP + sp_size * context_rows
     bias = jnp.transpose(offset_bias, (1, 0, 2))
@@ -531,7 +574,7 @@
             vmem((context_rows, depth), BF16),
             vmem((context_rows + 16, depth), BF16),
             vmem((tokens, depth), BF16),
-            vmem((big + 16, depth), BF16),
+            vmem((group_tokens + 16, depth), BF16),
             vmem((depth, 3 * width), BF16),
             vmem(out_weight.shape, BF16),
             vmem((2, piece_cols), F32),
@@ -541,6 +584,7 @@
             vmem((1, piece_cols), F32),
             vmem((ranks, 1, piece_cols), F32),
             vmem((4, depth), F32),
+            vmem((1, 3 * width), F32),
             vmem((tokens, LANES), F32),
             vmem((tokens, width), BF16),
             vmem((tokens + 2 * HALO * GRID_W, 2 * width), BF16),

time: 33.8 us -> 32.6 us (0.964)
  the two profiles are of different devices: /device:TPU:19 before, /device:TPU:0 now
where the time goes in v3:
time: 32.6 us; the launch traced here: 32.4 us
  Pallas kernels  31.3 us (96%)
  local copies, waits for them, and re-layouts  1.15 us (4%)
    pallas_call x1, Pallas kernels, local(): pl.pallas_call(kernel, in_specs=[hbm] * 13, out_specs=pl.BlockSpec(memory...  31.3 us
    unnamed x1, local copies, waits for them, and re-layouts  1.15 us

profile of v3, /device:TPU:0, one launch (start us, length us, event | category | flops | bytes accessed | tf_op | source)
XLA Modules:
  0.0 32.4 jit_solution(11214191552022226875)
XLA Ops:
  0.0 31.3 %shard_map.127 = bf16[384,2048]{1,0:T(8,128)(2,1)S(1)} custom-call(bf16[2048]{0:T(1024)(128)(2,1)} %cond_hbm.1, bf16[2048]{0:T(1024)(128)(2,1)} %ctxcond_hbm.1, bf16[2048]{0:T(1024)(128)(2,1)} %gain_hbm.1, bf16[512,512]{1,0:T(8,128)(2,1)} %shift_hbm.1, bf16[512,512]{1,0:T(8,128)(2,1)} %scale_hbm.1, bf16[512,512]{1,0:T(8,128)(2,1)} %gate_hbm.1, ...), custom_call_target="tpu_custom_call" | custom-call | flops 4831838208 | bytes 11010048 | tf_op jit(solution)/shard_map/pallas_call | solution.py:562
  31.3 1.1 %copy.15 = bf16[384,2048]{1,0:T(8,128)(2,1)} copy(bf16[384,2048]{1,0:T(8,128)(2,1)S(1)} %shard_map.127) | data formatting | bytes 3145728

commit v4 on v3

--- a/solution.py
+++ b/solution.py
@@ -90,7 +90,7 @@
     out_ref,
     cond, ctxcond, gain, small, modw, bias, braw, table, ctx, cblk, lat, xs, wqkv, wo,
     cterms, carrived, terms, arrived, gterms, garrived, vectors, added, inv, q_s, kv, ctx_kv,
-    scores, probs, stage, recv, acc,
+    scores, probs, partial, stats, stage, recv, acc,
     load_sem, lat_sem, cterm_send, cterm_recv, term_send, term_recv, gate_send, gate_recv,
     halo_send, halo_recv, ctx_send, ctx_recv, piece_send, piece_recv,
 ):
@@ -176,16 +176,20 @@
     arrived[me] = terms[...]
     garrived[me] = gterms[...]
 
+    def wait_all(slots, send, recv_sem):
+        all_but_one = slots.at[pl.ds(0, ranks - 1)]
+        to_peer(all_but_one, all_but_one, send, recv_sem, **peer(1)).wait()
+
     def cterm_copy(d):
         return to_peer(
-            cterms, carrived.at[me], cterm_send.at[d], cterm_recv.at[d], **peer(d)
+            cterms, carrived.at[me], cterm_send, cterm_recv, **peer(d)
         )
 
     def term_copy(d):
-        return to_peer(terms, arrived.at[me], term_send.at[d], term_recv.at[d], **peer(d))
+        return to_peer(terms, arrived.at[me], term_send, term_recv, **peer(d))
 
     def gate_copy(d):
-        return to_peer(gterms, garrived.at[me], gate_send.at[d], gate_recv.at[d], **peer(d))
+        return to_peer(gterms, garrived.at[me], gate_send, gate_recv, **peer(d))
 
     load_bias.wait()
     build_tables(bias, braw, table, heads)
@@ -237,9 +241,7 @@
                 total = total + ref[s * tp_size + t]
             vectors[rows, t * piece_cols : (t + 1) * piece_cols] = total
 
-    @pl.loop(1, ranks)
-    def _(d):
-        cterm_copy(d).wait()
+    wait_all(carrived, cterm_send, cterm_recv)
 
     sum_terms(carrived, slice(0, 2))
     row16 = lax.broadcasted_iota(jnp.int32, (16, depth), 0)
@@ -254,7 +256,7 @@
 
     def ctx_copy(d):
         return to_peer(
-            ctx_kv.at[ctx_place], ctx_kv.at[ctx_place], ctx_send.at[d], ctx_recv.at[d],
+            ctx_kv.at[ctx_place], ctx_kv.at[ctx_place], ctx_send, ctx_recv,
             sp=(sp + d) % sp_size, tp=tp,
         )
 
@@ -271,9 +273,7 @@
         halo_send.at[1], halo_recv.at[1], sp=jnp.minimum(sp + 1, sp_size - 1),
     )
 
-    @pl.loop(1, ranks)
-    def _(d):
-        term_copy(d).wait()
+    wait_all(arrived, term_send, term_recv)
 
     sum_terms(arrived, slice(2, 4))
     factor = (small[2:3, :] * (1.0 + vectors[3:4, :])).astype(BF16)
@@ -387,31 +387,76 @@
             probs[b, rows, :] = p.astype(BF16)
         return [1.0 / total for total in sums]
 
+    def merge(column, row=None):
+        parts = []
+        for c in range(width // LANES):
+            low, high = 2 * c, 2 * c + 1
+            if row is not None:
+                lanes = slice(c * LANES, (c + 1) * LANES)
+                first = row[low * size : (low + 1) * size, lanes]
+                second = row[high * size : (high + 1) * size, lanes]
+                if column is not None:
+                    first, second = first * column[low], second * column[high]
+            else:
+                first, second = column[low], column[high]
+            parts.append(jnp.where(first_head, first, second))
+        return jnp.concatenate(parts, axis=1)
+
+    def place_merged(g, b, merged):
+        merged = merged.astype(BF16)
+        for r, place in enumerate(places(g, b)):
+            stage[place, :] = merged[r * BLOCK : (r + 1) * BLOCK]
+
     def mix(g, b, inverses):
         values = jnp.concatenate(
             [kv[s, width:] for s in strips(g, b)] + [ctx_kv[:, width:]], axis=0
         )
         mixed = jnp.dot(probs[b], values, preferred_element_type=F32)
-        parts = []
-        for c in range(width // LANES):
-            h, lanes = 2 * c, slice(c * LANES, (c + 1) * LANES)
-            parts.append(
-                jnp.where(
-                    first_head,
-                    mixed[h * size : (h + 1) * size, lanes] * inverses[h],
-                    mixed[(h + 1) * size : (h + 2) * size, lanes] * inverses[h + 1],
-                )
+        place_merged(g, b, merge(inverses, mixed))
+
+    def head_rows(h):
+        return slice(h * size, (h + 1) * size)
+
+    def attend_near(g, b, slot):
+        for h in range(heads):
+            s = scores[b, head_rows(h), :near_keys]
+            peak = jnp.max(s, axis=1, keepdims=True)
+            p = jnp.exp2(s - peak)
+            spread = (size, LANES)
+            stats[slot, b, 0, head_rows(h), :] = jnp.broadcast_to(peak, spread)
+            stats[slot, b, 1, head_rows(h), :] = jnp.broadcast_to(
+                jnp.sum(p, axis=1, keepdims=True), spread
             )
-        merged = jnp.concatenate(parts, axis=1).astype(BF16)
-        for r, place in enumerate(places(g, b)):
-            stage[place, :] = merged[r * BLOCK : (r + 1) * BLOCK]
+            probs[b, head_rows(h), :near_keys] = p.astype(BF16)
+        values = jnp.concatenate([kv[s, width:] for s in strips(g, b)], axis=0)
+        mixed = jnp.dot(probs[b, :, :near_keys], values, preferred_element_type=F32)
+        partial[slot, b] = merge(None, mixed)
+
+    def attend_far(g, b, slot):
+        keeps, inverses = [], []
+        for h in range(heads):
+            old = stats[slot, b, 0, head_rows(h), :]
+            s = scores[b, head_rows(h), near_keys:]
+            peak = jnp.maximum(old, jnp.max(s, axis=1, keepdims=True))
+            p = jnp.exp2(s - jnp.concatenate([peak] * (s.shape[1] // LANES), axis=1))
+            keep = jnp.exp2(old - peak)
+            total = stats[slot, b, 1, head_rows(h), :] * keep
+            total = total + jnp.sum(p, axis=1, keepdims=True)
+            inverse = 1.0 / total
+            inverses.append(inverse)
+            keeps.append(keep * inverse)
+            probs[b, head_rows(h), near_keys:] = p.astype(BF16)
+        mixed = jnp.dot(
+            probs[b, :, near_keys:], ctx_kv[:, width:], preferred_element_type=F32
+        )
+        place_merged(g, b, partial[slot, b] * merge(keeps) + merge(inverses, mixed))
 
     def piece_copy(index):
         owner, p = index // pieces, index % pieces
         return to_peer(
             stage.at[pl.ds(aligned(index, piece), piece)],
             recv.at[tp, pl.ds(aligned(p, piece), piece)],
-            piece_send.at[index], piece_recv.at[tp, p], tp=owner,
+            piece_send, piece_recv.at[tp, p], tp=owner,
         )
 
     half = groups // 2
@@ -428,32 +473,34 @@
             def _():
                 piece_copy(index).start()
 
-    for b in range(blocks):
-        score_near(group_of(False, 0), b)
-
-    @pl.loop(1, sp_size)
-    def _(d):
-        ctx_copy(d).wait()
-
     @pl.loop(0, inner)
     def _(k):
-        g, following = group_of(False, k), group_of(False, jnp.minimum(k + 1, inner - 1))
-        score_far(g, 0)
+        g = group_of(False, k)
+        score_near(g, 0)
         for b in range(blocks):
             if b + 1 < blocks:
-                score_far(g, b + 1)
-            inverses = soften(b)
-            score_near(following, b)
-            mix(g, b, inverses)
+                score_near(g, b + 1)
+            attend_near(g, b, k)
+
+    others = ctx_kv.at[pl.ds(0, (sp_size - 1) * context_rows)]
+    to_peer(others, others, ctx_send, ctx_recv, sp=(sp + 1) % sp_size).wait()
+
+    @pl.loop(0, inner)
+    def _(k):
+        g = group_of(False, k)
+        for b in range(blocks):
+            score_far(g, b)
+        for b in range(blocks):
+            attend_far(g, b, k)
         send_pieces(g)
 
     project(unit(groups - 1), False)
 
     @pl.loop(0, groups - inner)
     def _(k):
-        edge = (k == 1) | (k == groups - inner - 1)
-        own = k != 1
-        j = jnp.where(edge, inner, jnp.where(k > 1, k - 1, k))
+        edge = (k == 2) | (k == groups - inner - 1)
+        own = k != 2
+        j = jnp.where(edge, inner, jnp.where(k > 2, k - 1, k))
         g = group_of(own, j)
 
         @pl.when((g == 0) & (sp > 0))
@@ -477,9 +524,7 @@
 
     load_wo.wait()
 
-    @pl.loop(1, ranks)
-    def _(d):
-        gate_copy(d).wait()
+    wait_all(garrived, gate_send, gate_recv)
 
     gates = []
     for t in range(tp_size):
@@ -495,7 +540,7 @@
     def arrival(source, p):
         rows = pl.ds(aligned(p, piece), piece)
         return to_peer(
-            stage.at[rows], recv.at[source, rows], piece_send.at[0],
+            stage.at[rows], recv.at[source, rows], piece_send,
             piece_recv.at[source, p], tp=source,
         )
 
@@ -511,12 +556,6 @@
         recv[tp, rows, :] = stage[pl.ds(aligned(tp * pieces + p, piece), piece), :]
         arrival(partner, p).wait_recv()
         acc[rows, :] = product(chip, rows)
-
-    @pl.loop(0, groups * per_group)
-    def _(index):
-        @pl.when(index // pieces != tp)
-        def _():
-            piece_copy(index).wait_send()
 
     @pl.loop(0, pieces)
     def _(k):
@@ -535,6 +574,9 @@
             turned.append(branch[r * GRID_W : (r + 1) * GRID_W - SHIFT])
         branch = jnp.concatenate(turned, axis=0)
         out_ref[rows, :] = (lat[own, :].astype(F32) + gate * branch).astype(BF16)
+
+    sent = stage.at[pl.ds(0, tokens - share)]
+    to_peer(sent, sent, piece_send, piece_recv.at[0, 0], tp=partner).wait_send()
 
 
 def local(
@@ -591,13 +633,13 @@
             vmem((sp_size * context_rows, 2 * width), BF16),
             vmem((GRID_W // BLOCK, stacked, keys), F32),
             vmem((GRID_W // BLOCK, stacked, keys), BF16),
+            vmem((groups // 2 - 1, GRID_W // BLOCK, GROUP * BLOCK, width), F32),
+            vmem((groups // 2 - 1, GRID_W // BLOCK, 2, stacked, LANES), F32),
             vmem((tokens, width), BF16),
             vmem((tp_size, share, width), BF16),
             vmem((share, depth), F32),
-            dma((12,)), dma((groups,)), dma((ranks,)), dma((ranks,)), dma((ranks,)),
-            dma((ranks,)), dma((ranks,)), dma((ranks,)), dma((2,)), dma((2,)),
-            dma((sp_size,)), dma((sp_size,)),
-            dma((tp_size * pieces,)), dma((tp_size, pieces)),
+            dma((12,)), dma((groups,)), dma, dma, dma, dma, dma, dma, dma((2,)), dma((2,)),
+            dma, dma, dma, dma((tp_size, pieces)),
         ],
         compiler_params=pltpu.CompilerParams(
             vmem_limit_bytes=60 * 2**20, collective_id=0, has_side_effects=True

time: 32.6 us -> 31.8 us (0.975)
  Pallas kernels: 31.3 us -> 30.4 us
    pallas_call x1, Pallas kernels: 31.3 us -> 30.4 us  [local(): pl.pallas_call(kernel, in_specs=[hbm] * 13, out_specs=pl.BlockSpec(memory...]
where the time goes in v4:
time: 31.8 us; the launch traced here: 31.6 us
  Pallas kernels  30.4 us (96%)
  local copies, waits for them, and re-layouts  1.15 us (4%)
    pallas_call x1, Pallas kernels, local(): pl.pallas_call(kernel, in_specs=[hbm] * 13, out_specs=pl.BlockSpec(memory...  30.4 us
    unnamed x1, local copies, waits for them, and re-layouts  1.15 us

profile of v4, /device:TPU:0, one launch (start us, length us, event | category | flops | bytes accessed | tf_op | source)
XLA Modules:
  0.0 31.6 jit_solution(7091731792890478856)
XLA Ops:
  0.0 30.4 %shard_map.127 = bf16[384,2048]{1,0:T(8,128)(2,1)S(1)} custom-call(bf16[2048]{0:T(1024)(128)(2,1)} %cond_hbm.1, bf16[2048]{0:T(1024)(128)(2,1)} %ctxcond_hbm.1, bf16[2048]{0:T(1024)(128)(2,1)} %gain_hbm.1, bf16[512,512]{1,0:T(8,128)(2,1)} %shift_hbm.1, bf16[512,512]{1,0:T(8,128)(2,1)} %scale_hbm.1, bf16[512,512]{1,0:T(8,128)(2,1)} %gate_hbm.1, ...), custom_call_target="tpu_custom_call" | custom-call | flops 4831838208 | bytes 11010048 | tf_op jit(solution)/shard_map/pallas_call | solution.py:604
  30.4 1.1 %copy.15 = bf16[384,2048]{1,0:T(8,128)(2,1)} copy(bf16[384,2048]{1,0:T(8,128)(2,1)S(1)} %shard_map.127) | data formatting | bytes 3145728

commit v5 on v4

--- a/solution.py
+++ b/solution.py
@@ -167,10 +167,12 @@
     own_inputs = pl.ds(aligned(sp, input_rows), input_rows)
     value = jnp.where(row8 == 0, small[0:1, own_inputs], small[1:2, own_inputs])
     act = (value / (1.0 + jnp.exp(-value))).astype(BF16)
+    products = []
     for i in range(2):
         both = jnp.dot(act, modw[i], preferred_element_type=F32)
-        terms[i : i + 1, :] = both[0:1]
-        cterms[i : i + 1, :] = both[1:2]
+        products.append(both)
+    cterms[...] = jnp.concatenate([both[1:2] for both in products], axis=0).astype(BF16)
+    terms[...] = jnp.concatenate([both[0:1] for both in products], axis=0).astype(BF16)
     gterms[...] = jnp.dot(act, modw[2], preferred_element_type=F32)[:1]
     carrived[me] = cterms[...]
     arrived[me] = terms[...]
@@ -236,9 +238,9 @@
 
     def sum_terms(ref, rows):
         for t in range(tp_size):
-            total = ref[t]
+            total = ref[t].astype(F32)
             for s in range(1, sp_size):
-                total = total + ref[s * tp_size + t]
+                total = total + ref[s * tp_size + t].astype(F32)
             vectors[rows, t * piece_cols : (t + 1) * piece_cols] = total
 
     wait_all(carrived, cterm_send, cterm_recv)
@@ -619,10 +621,10 @@
             vmem((group_tokens + 16, depth), BF16),
             vmem((depth, 3 * width), BF16),
             vmem(out_weight.shape, BF16),
-            vmem((2, piece_cols), F32),
-            vmem((ranks, 2, piece_cols), F32),
-            vmem((2, piece_cols), F32),
-            vmem((ranks, 2, piece_cols), F32),
+            vmem((2, piece_cols), BF16),
+            vmem((ranks, 2, piece_cols), BF16),
+            vmem((2, piece_cols), BF16),
+            vmem((ranks, 2, piece_cols), BF16),
             vmem((1, piece_cols), F32),
             vmem((ranks, 1, piece_cols), F32),
             vmem((4, depth), F32),

time: 31.8 us -> 31.2 us (0.981)
  Pallas kernels: 30.4 us -> 29.8 us
    pallas_call x1, Pallas kernels: 30.4 us -> 29.8 us  [local(): pl.pallas_call(kernel, in_specs=[hbm] * 13, out_specs=pl.BlockSpec(memory...]
where the time goes in v5:
time: 31.2 us; the launch traced here: 31 us
  Pallas kernels  29.8 us (96%)
  local copies, waits for them, and re-layouts  1.15 us (4%)
    pallas_call x1, Pallas kernels, local(): pl.pallas_call(kernel, in_specs=[hbm] * 13, out_specs=pl.BlockSpec(memory...  29.8 us
    unnamed x1, local copies, waits for them, and re-layouts  1.15 us

profile of v5, /device:TPU:0, one launch (start us, length us, event | category | flops | bytes accessed | tf_op | source)
XLA Modules:
  0.0 31.0 jit_solution(1239727566849278365)
XLA Ops:
  0.0 29.8 %shard_map.127 = bf16[384,2048]{1,0:T(8,128)(2,1)S(1)} custom-call(bf16[2048]{0:T(1024)(128)(2,1)} %cond_hbm.1, bf16[2048]{0:T(1024)(128)(2,1)} %ctxcond_hbm.1, bf16[2048]{0:T(1024)(128)(2,1)} %gain_hbm.1, bf16[512,512]{1,0:T(8,128)(2,1)} %shift_hbm.1, bf16[512,512]{1,0:T(8,128)(2,1)} %scale_hbm.1, bf16[512,512]{1,0:T(8,128)(2,1)} %gate_hbm.1, ...), custom_call_target="tpu_custom_call" | custom-call | flops 4831838208 | bytes 11010048 | tf_op jit(solution)/shard_map/pallas_call | solution.py:606
  29.8 1.1 %copy.15 = bf16[384,2048]{1,0:T(8,128)(2,1)} copy(bf16[384,2048]{1,0:T(8,128)(2,1)S(1)} %shard_map.127) | data formatting | bytes 3145728

commit v6 on v5

--- a/solution.py
+++ b/solution.py
@@ -279,7 +279,7 @@
 
     sum_terms(arrived, slice(2, 4))
     factor = (small[2:3, :] * (1.0 + vectors[3:4, :])).astype(BF16)
-    xs[group_tokens:, :] = jnp.where(row16 == 0, vectors[2:3, :], 0.0).astype(BF16)
+    xs[group_tokens : group_tokens + 16, :] = jnp.where(row16 == 0, vectors[2:3, :], 0.0).astype(BF16)
 
     upper = tp * 2 >= tp_size
 
@@ -290,23 +290,26 @@
             return jnp.where(upper, groups - 2, 1)
         return jnp.where(upper, k - 1, k + 1)
 
-    def project(i, first):
-        rows = pl.ds(aligned(i, group_tokens), group_tokens)
-        place = pl.ds(aligned(i, group_tokens) + halo, group_tokens)
-        xs[:group_tokens, :] = lat[rows, :] * factor
+    def project(i, first, span=1):
+        step = span * group_tokens
+        rows = pl.ds(aligned(i, group_tokens), step)
+        place = pl.ds(aligned(i, group_tokens) + halo, step)
+        xs[:step, :] = lat[rows, :] * factor
         scale = jnp.concatenate([inv[rows, :]] * (width // LANES), axis=1)
 
         def part(n):
             columns = slice(n * width, (n + 1) * width)
-            left = xs[...] if first else xs[:group_tokens, :]
-            y = jnp.dot(left, wqkv[:, columns], preferred_element_type=F32)
+            y = jnp.dot(
+                xs[: step + 16 if first else step, :], wqkv[:, columns],
+                preferred_element_type=F32,
+            )
             if first:
-                added[0:1, columns] = y[group_tokens : group_tokens + 1]
-            return y[:group_tokens] * scale + added[0:1, columns]
+                added[0:1, columns] = y[step : step + 1]
+            return y[:step] * scale + added[0:1, columns]
 
         q = part(0) * (HEAD_DIM**-0.5 * LOG2E)
         turned = []
-        for r in range(GROUP):
+        for r in range(span * GROUP):
             turned.append(q[r * GRID_W + SHIFT : (r + 1) * GRID_W])
             turned.append(q[r * GRID_W : r * GRID_W + SHIFT])
         q_s[rows, :] = jnp.concatenate(turned, axis=0).astype(BF16)
@@ -315,15 +318,17 @@
 
     project(unit(0), True)
 
-    @pl.loop(1, groups - 1)
+    steps = (groups - 2) // 2
+
+    @pl.loop(0, steps)
     def _(k):
-        project(jnp.where(upper, k - 1, k + 1), False)
-
-        @pl.when((k == 1) & (sp > 0))
+        project(jnp.where(upper, 2 * k, 2 * k + 2), False, 2)
+
+        @pl.when((k == steps - 1) & (sp > 0))
         def _():
             down.start()
 
-        @pl.when((k == groups - 2) & (sp < sp_size - 1))
+        @pl.when((k == steps - 1) & (sp < sp_size - 1))
         def _():
             up.start()
 
@@ -465,7 +470,9 @@
     inner = half - 1
 
     def group_of(own, j):
-        return jnp.where(upper != own, (j + 1) % half, half + j)
+        early = jnp.where(j == 0, 0, jnp.where(j == 1, inner, j - 1))
+        low = (jnp.where(sp == 0, early, j) + 1) % half
+        return jnp.where(upper != own, low, half + j)
 
     def send_pieces(g):
         for n in range(per_group):
@@ -498,12 +505,13 @@
 
     project(unit(groups - 1), False)
 
+    no_halo = jnp.where(upper, sp == 0, sp == sp_size - 1)
+    turn = jnp.where(no_halo, 0, jnp.where(sp == 0, groups - inner - 1, inner))
+
     @pl.loop(0, groups - inner)
     def _(k):
-        edge = (k == 2) | (k == groups - inner - 1)
-        own = k != 2
-        j = jnp.where(edge, inner, jnp.where(k > 2, k - 1, k))
-        g = group_of(own, j)
+        own = k != turn
+        g = group_of(own, jnp.where(own, k - jnp.where(k > turn, 1, 0), inner))
 
         @pl.when((g == 0) & (sp > 0))
         def _():
@@ -552,8 +560,12 @@
             pair, wo[pl.ds(aligned(c, 2 * width), 2 * width), :], preferred_element_type=F32
         )
 
+    def landing(k):
+        return jnp.where(tp == 0, (k + per_group) % pieces, k)
+
     @pl.loop(0, pieces)
-    def _(p):
+    def _(k):
+        p = landing(k)
         rows = pl.ds(aligned(p, piece), piece)
         recv[tp, rows, :] = stage[pl.ds(aligned(tp * pieces + p, piece), piece), :]
         arrival(partner, p).wait_recv()
@@ -561,7 +573,7 @@
 
     @pl.loop(0, pieces)
     def _(k):
-        p = jnp.where(tp == 0, (k + per_group) % pieces, k)
+        p = landing(k)
         rows = pl.ds(aligned(p, piece), piece)
         own = pl.ds(aligned(tp * pieces + p, piece), piece)
         branch = acc[rows, :]
@@ -618,7 +630,7 @@
             vmem((context_rows, depth), BF16),
             vmem((context_rows + 16, depth), BF16),
             vmem((tokens, depth), BF16),
-            vmem((group_tokens + 16, depth), BF16),
+            vmem((2 * group_tokens, depth), BF16),
             vmem((depth, 3 * width), BF16),
             vmem(out_weight.shape, BF16),
             vmem((2, piece_cols), BF16),

time: 31.2 us -> 30.2 us (0.968)
  Pallas kernels: 29.8 us -> 28.8 us
    pallas_call x1, Pallas kernels: 29.8 us -> 28.8 us  [local(): pl.pallas_call(kernel, in_specs=[hbm] * 13, out_specs=pl.BlockSpec(memory...]
where the time goes in v6:
time: 30.2 us; the launch traced here: 30 us
  Pallas kernels  28.8 us (95%)
  local copies, waits for them, and re-layouts  1.15 us (4%)
    pallas_call x1, Pallas kernels, local(): pl.pallas_call(kernel, in_specs=[hbm] * 13, out_specs=pl.BlockSpec(memory...  28.8 us
    unnamed x1, local copies, waits for them, and re-layouts  1.15 us

profile of v6, /device:TPU:0, one launch (start us, length us, event | category | flops | bytes accessed | tf_op | source)
XLA Modules:
  0.0 30.0 jit_solution(1730949546254956110)
XLA Ops:
  0.0 28.8 %shard_map.127 = bf16[384,2048]{1,0:T(8,128)(2,1)S(1)} custom-call(bf16[2048]{0:T(1024)(128)(2,1)} %cond_hbm.1, bf16[2048]{0:T(1024)(128)(2,1)} %ctxcond_hbm.1, bf16[2048]{0:T(1024)(128)(2,1)} %gain_hbm.1, bf16[512,512]{1,0:T(8,128)(2,1)} %shift_hbm.1, bf16[512,512]{1,0:T(8,128)(2,1)} %scale_hbm.1, bf16[512,512]{1,0:T(8,128)(2,1)} %gate_hbm.1, ...), custom_call_target="tpu_custom_call" | custom-call | flops 4831838208 | bytes 11010048 | tf_op jit(solution)/shard_map/pallas_call | solution.py:618
  28.8 1.1 %copy.15 = bf16[384,2048]{1,0:T(8,128)(2,1)} copy(bf16[384,2048]{1,0:T(8,128)(2,1)S(1)} %shard_map.127) | data formatting | bytes 3145728

commit v7 on v6

--- a/solution.py
+++ b/solution.py
@@ -485,10 +485,9 @@
     @pl.loop(0, inner)
     def _(k):
         g = group_of(False, k)
-        score_near(g, 0)
         for b in range(blocks):
-            if b + 1 < blocks:
-                score_near(g, b + 1)
+            score_near(g, b)
+        for b in range(blocks):
             attend_near(g, b, k)
 
     others = ctx_kv.at[pl.ds(0, (sp_size - 1) * context_rows)]
@@ -523,12 +522,10 @@
             up.wait_send()
             down.wait_recv()
 
-        score_near(g, 0)
-        score_far(g, 0)
         for b in range(blocks):
-            if b + 1 < blocks:
-                score_near(g, b + 1)
-                score_far(g, b + 1)
+            score_near(g, b)
+            score_far(g, b)
+        for b in range(blocks):
             mix(g, b, soften(b))
         send_pieces(g)
 

time: 30.2 us -> 29.8 us (0.987)
  Pallas kernels: 28.8 us -> 28.4 us
    pallas_call x1, Pallas kernels: 28.8 us -> 28.4 us  [local(): pl.pallas_call(kernel, in_specs=[hbm] * 13, out_specs=pl.BlockSpec(memory...]
where the time goes in v7:
time: 29.8 us; the launch traced here: 29.6 us
  Pallas kernels  28.4 us (95%)
  local copies, waits for them, and re-layouts  1.15 us (4%)
    pallas_call x1, Pallas kernels, local(): pl.pallas_call(kernel, in_specs=[hbm] * 13, out_specs=pl.BlockSpec(memory...  28.4 us
    unnamed x1, local copies, waits for them, and re-layouts  1.15 us

profile of v7, /device:TPU:0, one launch (start us, length us, event | category | flops | bytes accessed | tf_op | source)
XLA Modules:
  0.0 29.6 jit_solution(3241501488581280315)
XLA Ops:
  0.0 28.4 %shard_map.127 = bf16[384,2048]{1,0:T(8,128)(2,1)S(1)} custom-call(bf16[2048]{0:T(1024)(128)(2,1)} %cond_hbm.1, bf16[2048]{0:T(1024)(128)(2,1)} %ctxcond_hbm.1, bf16[2048]{0:T(1024)(128)(2,1)} %gain_hbm.1, bf16[512,512]{1,0:T(8,128)(2,1)} %shift_hbm.1, bf16[512,512]{1,0:T(8,128)(2,1)} %scale_hbm.1, bf16[512,512]{1,0:T(8,128)(2,1)} %gate_hbm.1, ...), custom_call_target="tpu_custom_call" | custom-call | flops 4831838208 | bytes 11010048 | tf_op jit(solution)/shard_map/pallas_call | solution.py:615
  28.4 1.1 %copy.15 = bf16[384,2048]{1,0:T(8,128)(2,1)} copy(bf16[384,2048]{1,0:T(8,128)(2,1)S(1)} %shard_map.127) | data formatting | bytes 3145728

commit v8 on v7

--- a/solution.py
+++ b/solution.py
@@ -125,16 +125,16 @@
         pltpu.make_async_copy(ctxcond_hbm, ctxcond, load_sem.at[1]),
         pltpu.make_async_copy(gain_hbm, gain, load_sem.at[2]),
         pltpu.make_async_copy(shift_hbm, modw.at[0], load_sem.at[3]),
-        pltpu.make_async_copy(scale_hbm, modw.at[1], load_sem.at[4]),
-        pltpu.make_async_copy(gate_hbm, modw.at[2], load_sem.at[5]),
+        pltpu.make_async_copy(scale_hbm, modw.at[1], load_sem.at[3]),
+        pltpu.make_async_copy(gate_hbm, modw.at[2], load_sem.at[3]),
     ]
-    load_bias = pltpu.make_async_copy(bias_hbm, bias, load_sem.at[6])
-    load_ctx = pltpu.make_async_copy(ctx_hbm, ctx, load_sem.at[7])
+    load_bias = pltpu.make_async_copy(bias_hbm, bias, load_sem.at[4])
+    load_ctx = pltpu.make_async_copy(ctx_hbm, ctx, load_sem.at[5])
     load_weights = [
-        pltpu.make_async_copy(w, wqkv.at[:, pl.ds(i * width, width)], load_sem.at[8 + i])
+        pltpu.make_async_copy(w, wqkv.at[:, pl.ds(i * width, width)], load_sem.at[6])
         for i, w in enumerate((wq_hbm, wk_hbm, wv_hbm))
     ]
-    load_wo = pltpu.make_async_copy(wo_hbm, wo, load_sem.at[11])
+    load_wo = pltpu.make_async_copy(wo_hbm, wo, load_sem.at[7])
 
     def load_lat(i):
         rows = pl.ds(aligned(i, group_tokens), group_tokens)
@@ -158,8 +158,9 @@
         load.start()
     load_wo.start()
 
-    for load in early:
+    for load in early[:3]:
         load.wait()
+    pltpu.make_async_copy(modw, modw, load_sem.at[3]).wait()
     small[0:1, :] = cond[...].astype(F32).reshape(1, depth)
     small[1:2, :] = ctxcond[...].astype(F32).reshape(1, depth)
     small[2:3, :] = gain[...].astype(F32).reshape(1, depth)
@@ -233,8 +234,7 @@
             rows = pl.ds(aligned(i, group_tokens) + r, 128)
             inv[rows, :] = jnp.broadcast_to(inverse_of(lat, rows), (128, LANES))
 
-    for load in load_weights:
-        load.wait()
+    pltpu.make_async_copy(wqkv, wqkv, load_sem.at[6]).wait()
 
     def sum_terms(ref, rows):
         for t in range(tp_size):
@@ -649,7 +649,7 @@
             vmem((tokens, width), BF16),
             vmem((tp_size, share, width), BF16),
             vmem((share, depth), F32),
-            dma((12,)), dma((groups,)), dma, dma, dma, dma, dma, dma, dma((2,)), dma((2,)),
+            dma((8,)), dma((groups,)), dma, dma, dma, dma, dma, dma, dma((2,)), dma((2,)),
             dma, dma, dma, dma((tp_size, pieces)),
         ],
         compiler_params=pltpu.CompilerParams(

time: 29.8 us -> 29.8 us (level)
  no operation moved by 1% of the time
where the time goes in v8:
time: 29.8 us; the launch traced here: 29.5 us
  Pallas kernels  28.4 us (95%)
  local copies, waits for them, and re-layouts  1.15 us (4%)
    pallas_call x1, Pallas kernels, local(): pl.pallas_call(kernel, in_specs=[hbm] * 13, out_specs=pl.BlockSpec(memory...  28.4 us
    unnamed x1, local copies, waits for them, and re-layouts  1.15 us

profile of v8, /device:TPU:0, one launch (start us, length us, event | category | flops | bytes accessed | tf_op | source)
XLA Modules:
  0.0 29.5 jit_solution(13744581612366871799)
XLA Ops:
  0.0 28.4 %shard_map.127 = bf16[384,2048]{1,0:T(8,128)(2,1)S(1)} custom-call(bf16[2048]{0:T(1024)(128)(2,1)} %cond_hbm.1, bf16[2048]{0:T(1024)(128)(2,1)} %ctxcond_hbm.1, bf16[2048]{0:T(1024)(128)(2,1)} %gain_hbm.1, bf16[512,512]{1,0:T(8,128)(2,1)} %shift_hbm.1, bf16[512,512]{1,0:T(8,128)(2,1)} %scale_hbm.1, bf16[512,512]{1,0:T(8,128)(2,1)} %gate_hbm.1, ...), custom_call_target="tpu_custom_call" | custom-call | flops 4831838208 | bytes 11010048 | tf_op jit(solution)/shard_map/pallas_call | solution.py:615
  28.4 1.1 %copy.15 = bf16[384,2048]{1,0:T(8,128)(2,1)} copy(bf16[384,2048]{1,0:T(8,128)(2,1)S(1)} %shard_map.127) | data formatting | bytes 3145728
